TPU v7x, 32 devices: a whole 2x2x4 slice. The times are simulated.
32 devices in a mesh: fs: 8 (over z, y), tp: 4 (over x, core).
Axes of the slice: x: 2, y: 2, z: 4, core: 2. Of those that a mesh axis runs over, the one named last changes fastest.
Arguments:
- tokens: bfloat16 [6144, 2048], P('fs', 'tp'), may hold values from -40 to 40
- gain_one: float32 [2048], P('tp'), may hold values from 0.1 to 1.9
- w_gate: float32 [2048, 3072], P('fs', 'tp'), may hold values from -0.125 to 0.125
- w_up: float32 [2048, 3072], P('fs', 'tp'), may hold values from -0.125 to 0.125
- w_down: float32 [3072, 2048], P('tp', 'fs'), may hold values from -0.109375 to 0.109375
- scale_gate: float32 [3072], P('tp'), may hold values from 0.5 to 2
- scale_up: float32 [3072], P('tp'), may hold values from 0.5 to 2
- scale_down: float32 [2048], P('tp'), may hold values from 0.5 to 2
- gain_mix: float32 [2048], P('tp'), may hold values from 0.1 to 1.9
- w_query: float32 [2048, 2048], P('fs', 'tp'), may hold values from -0.125 to 0.125
- w_key: float32 [2048, 2048], P('fs', 'tp'), may hold values from -0.125 to 0.125
- w_value: float32 [2048, 2048], P('fs', 'tp'), may hold values from -0.125 to 0.125
- w_outgate: float32 [2048, 2048], P('fs', 'tp'), may hold values from -0.125 to 0.125
- scale_query: float32 [2048], P('tp'), may hold values from 0.5 to 2
- scale_key: float32 [2048], P('tp'), may hold values from 0.5 to 2
- scale_value: float32 [2048], P('tp'), may hold values from 0.5 to 2
- scale_outgate: float32 [2048], P('tp'), may hold values from 0.5 to 2
- ret_gain: float32 [2048], P('tp'), may hold values from 0.1 to 1.9
- decay_rate: float32 [8], P('tp'), may hold values from 0 to 2
- w_mix: float32 [2048, 2048], P('tp', 'fs'), may hold values from -0.125 to 0.125
- scale_mix: float32 [2048], P('tp'), may hold values from 0.5 to 2
- gain_two: float32 [2048], P('tp'), may hold values from 0.1 to 1.9
Outputs:
- layer_out: bfloat16 [6144, 2048], P('fs', 'tp')
All inputs are finite; a program needn't handle non-finite values.
Results may differ from a plain program's by a relative error of at most 0.022.
Values may be sent and summed in bfloat16 or wider, within the bound.
A program may use at most 128 MiB of HBM per device.

v0:
```python
import jax
import jax.numpy as jnp
from jax import lax
from jax.sharding import PartitionSpec as P

D = 2048
LEN = 256
BLK = 128


EPS = 1e-06
HEAD_EPS = 0.1


def rotate_pairs(values):
    paired = values.reshape(values.shape[:-1] + (values.shape[-1] // 2, 2))
    return jnp.stack((-paired[..., 1], paired[..., 0]), axis=-1).reshape(values.shape)


def retain(query_rows, key_rows, value_rows, decay_rate, length, block):
    highest = lax.Precision.HIGHEST
    total_rows = query_rows.shape[0]
    heads = decay_rate.shape[0]
    head_size = query_rows.shape[1] // heads
    sequences = total_rows // length
    nblocks = length // block

    def split_heads(values):
        return values.astype(jnp.float32).reshape(sequences, length, heads, head_size)

    freq = 1.0 / 10000.0 ** jnp.linspace(0.0, 1.0, head_size // 2, dtype=jnp.float32)
    freq = jnp.repeat(freq, 2)
    angles = jnp.arange(length, dtype=jnp.float32)[:, None] * freq[None, :]
    sines = jnp.sin(angles)[None, :, None, :]
    cosines = jnp.cos(angles)[None, :, None, :]
    queries = split_heads(query_rows)
    queries = queries * cosines + rotate_pairs(queries) * sines
    keys_all = split_heads(key_rows) * head_size ** (-0.5)
    keys_all = keys_all * cosines + rotate_pairs(keys_all) * sines
    values_all = split_heads(value_rows)
    log_decay = -decay_rate
    offsets = jnp.arange(block, dtype=jnp.float32)
    distance = offsets[:, None] - offsets[None, :]
    inside = jnp.where(
        distance >= 0, jnp.exp(log_decay[:, None, None] * jnp.maximum(distance, 0.0)), 0.0
    )
    query_decay = jnp.exp(log_decay[None, :] * (offsets[:, None] + 1.0))
    key_decay = jnp.exp(log_decay[None, :] * (block - 1.0 - offsets[:, None]))
    block_decay = jnp.exp(log_decay * block)

    def to_blocks(values):
        return jnp.moveaxis(values.reshape(sequences, nblocks, block, heads, head_size), 1, 0)

    def advance(carried, pieces):
        query_blk, key_blk, value_blk = pieces
        scores = jnp.einsum("snhd,smhd->shnm", query_blk, key_blk, precision=highest) * inside
        within = jnp.einsum("shnm,smhe->snhe", scores, value_blk, precision=highest)
        across = (
            jnp.einsum("snhd,shde->snhe", query_blk, carried, precision=highest)
            * query_decay[None, :, :, None]
        )
        weighted = key_blk * key_decay[None, :, :, None]
        carried = carried * block_decay[None, :, None, None] + jnp.einsum(
            "smhd,smhe->shde", weighted, value_blk, precision=highest
        )
        return (carried, within + across)

    initial = jnp.zeros((sequences, heads, head_size, head_size), jnp.float32)
    _, results = lax.scan(
        advance, initial, (to_blocks(queries), to_blocks(keys_all), to_blocks(values_all))
    )
    results = jnp.moveaxis(results, 0, 1).reshape(sequences, length, heads, head_size)
    results = results * lax.rsqrt(jnp.mean(results * results, axis=-1, keepdims=True) + HEAD_EPS)
    return results.reshape(total_rows, heads * head_size)


def normed_rows(hidden_in, norm_gain):
    widened = hidden_in.astype(jnp.float32)
    totals = lax.psum(jnp.sum(widened * widened, axis=1), "tp")
    scaled = widened * lax.rsqrt(totals / D + EPS)[:, None] * norm_gain
    return lax.all_gather(scaled.astype(jnp.bfloat16), "tp", axis=1, tiled=True)


def summed_share(partial_value):
    rounded = lax.optimization_barrier(partial_value.astype(jnp.bfloat16))
    return lax.psum_scatter(
        rounded.astype(jnp.float32).astype(jnp.bfloat16), "tp", scatter_dimension=1, tiled=True
    ).astype(jnp.float32)


def ffn_gathered(features, gate_low, up_low, down_low, scale_gate, scale_up):
    gate_add = jnp.dot(
        features,
        lax.all_gather(gate_low, "fs", axis=0, tiled=True),
        preferred_element_type=jnp.float32,
    )
    up_add = jnp.dot(
        features,
        lax.all_gather(up_low, "fs", axis=0, tiled=True),
        preferred_element_type=jnp.float32,
    )
    hidden = (jax.nn.silu(gate_add * scale_gate) * (up_add * scale_up)).astype(jnp.bfloat16)
    return jnp.dot(
        hidden,
        lax.all_gather(down_low, "fs", axis=1, tiled=True),
        preferred_element_type=jnp.float32,
    )


def per_device(
    tokens,
    gain_one,
    w_gate,
    w_up,
    w_down,
    scale_gate,
    scale_up,
    scale_down,
    gain_mix,
    w_query,
    w_key,
    w_value,
    w_outgate,
    scale_query,
    scale_key,
    scale_value,
    scale_outgate,
    ret_gain,
    decay_rate,
    w_mix,
    scale_mix,
    gain_two,
):
    norm_one, norm_mix, norm_two, down_cols, mix_cols = (
        gain_one,
        gain_mix,
        gain_two,
        scale_down,
        scale_mix,
    )
    gate_low = w_gate.astype(jnp.bfloat16)
    up_low = w_up.astype(jnp.bfloat16)
    down_low = w_down.astype(jnp.bfloat16)
    ffn_one = ffn_gathered(
        normed_rows(tokens, norm_one), gate_low, up_low, down_low, scale_gate, scale_up
    )
    first = (tokens.astype(jnp.float32) + 0.5 * summed_share(ffn_one) * down_cols).astype(
        jnp.bfloat16
    )
    features = normed_rows(first, norm_mix)
    pieces = (
        lax.all_gather(w_query.astype(jnp.bfloat16), "fs", axis=0, tiled=True),
        lax.all_gather(w_key.astype(jnp.bfloat16), "fs", axis=0, tiled=True),
        lax.all_gather(w_value.astype(jnp.bfloat16), "fs", axis=0, tiled=True),
        lax.all_gather(w_outgate.astype(jnp.bfloat16), "fs", axis=0, tiled=True),
    )
    query_pre, key_pre, value_pre, outgate_pre = tuple(
        (jnp.dot(features, piece, preferred_element_type=jnp.float32) for piece in pieces)
    )
    query_rows = (query_pre * scale_query).astype(jnp.bfloat16)
    key_rows = (key_pre * scale_key).astype(jnp.bfloat16)
    value_rows = (value_pre * scale_value).astype(jnp.bfloat16)
    outgate_rows = (outgate_pre * scale_outgate).astype(jnp.bfloat16)
    retained = retain(query_rows, key_rows, value_rows, decay_rate, LEN, BLK)
    mixed = (retained * ret_gain * jax.nn.silu(outgate_rows.astype(jnp.float32))).astype(
        jnp.bfloat16
    )
    mix_partial = jnp.dot(
        mixed,
        lax.all_gather(w_mix.astype(jnp.bfloat16), "fs", axis=1, tiled=True),
        preferred_element_type=jnp.float32,
    )
    second = (first.astype(jnp.float32) + summed_share(mix_partial) * mix_cols).astype(jnp.bfloat16)
    ffn_two = ffn_gathered(
        normed_rows(second, norm_two), gate_low, up_low, down_low, scale_gate, scale_up
    )
    result = (second.astype(jnp.float32) + 0.5 * summed_share(ffn_two) * down_cols).astype(
        jnp.bfloat16
    )
    return result


def solution(mesh):
    return jax.shard_map(
        per_device,
        mesh=mesh,
        in_specs=(
            P("fs", "tp"),
            P("tp"),
            P("fs", "tp"),
            P("fs", "tp"),
            P("tp", "fs"),
            P("tp"),
            P("tp"),
            P("tp"),
            P("tp"),
            P("fs", "tp"),
            P("fs", "tp"),
            P("fs", "tp"),
            P("fs", "tp"),
            P("tp"),
            P("tp"),
            P("tp"),
            P("tp"),
            P("tp"),
            P("tp"),
            P("tp", "fs"),
            P("tp"),
            P("tp"),
        ),
        out_specs=P("fs", "tp"),
        check_vma=False,
    )
```

profile of v0, /device:TPU:0, one launch (start us, length us, event | category | flops | bytes accessed | tf_op | source)
XLA Modules:
  0.0 711.0 jit_solution(11164169633599705700)
XLA Ops:
  8.0 8.4 %psum.21 = f32[768]{0:T(1024)S(1)} all-reduce(f32[768]{0:T(1024)S(1)} %fusion.31), channel_id=1, replica_groups=mesh['fs'=8,'tp'=4] {'tp'}, use_global_device_ids=true, to_apply=%region_1.0 | all-reduce | flops 768 | bytes 6144 | tf_op jit(solution)/shard_map/psum | solution.py:79
  21.7 26.0 %all-gather.12.cloned.1.call-done = bf16[768,2048]{1,0:T(8,128)(2,1)} async-done(((bf16[768,512]{1,0:T(8,128)(2,1)}), bf16[768,2048]{1,0:T(8,128)(2,1)}) %all-gather.12.cloned.1.call-update) | async-done | bytes 3145744 | tf_op jit(solution)/shard_map/all_gather | solution.py:81
  47.6 62.2 %all-gather.14.cloned.1.call-done = bf16[2048,768]{1,0:T(8,128)(2,1)} async-done(((bf16[256,768]{1,0:T(8,128)(2,1)}), bf16[2048,768]{1,0:T(8,128)(2,1)}) %all-gather.14.cloned.1.call-update) | async-done | bytes 3145744 | tf_op jit(solution)/shard_map/all_gather | solution.py:94
  109.9 6.9 fusion.60
  116.7 54.0 %all-gather.16.cloned.1.call-done = bf16[2048,768]{1,0:T(8,128)(2,1)} async-done(((bf16[256,768]{1,0:T(8,128)(2,1)}), bf16[2048,768]{1,0:T(8,128)(2,1)}) %all-gather.16.cloned.1.call-update) | async-done | bytes 3145744 | tf_op jit(solution)/shard_map/all_gather | solution.py:99
  170.8 63.2 %all-gather.18.cloned.1.call-done = bf16[768,2048]{1,0:T(8,128)(2,1)} async-done(((bf16[768,256]{1,0:T(8,128)(2,1)}), bf16[768,2048]{1,0:T(8,128)(2,1)}) %all-gather.18.cloned.1.call-update) | async-done | bytes 3145744 | tf_op jit(solution)/shard_map/all_gather | solution.py:105
  234.0 11.0 %convolution_convert_fusion.2 = bf16[768,2048]{1,0:T(8,128)(2,1)} fusion(bf16[768,2048]{1,0:T(8,128)(2,1)} %all-gather.18.cloned.1.call-done, f32[768,768]{1,0:T(8,128)} %fusion.60, bf16[768,2048]{1,0:T(8,128)(2,1)S(1)} %copy-done.28, bf16[2048,768]{1,0:T(8,128)(2,1)} %all-gather.16.cloned.1.call-done, f32[768]{0:T(1024)S(1)} %copy-done.29, ...), kind=kOutput, calls=%fused_computation.31 | convolution fusion | flops 4838129664 | bytes 14948352 | tf_op jit(solution)/shard_map/dot_general | solution.py:103
  246.9 34.2 %reduce-scatter.4.cloned.1.call-done = bf16[768,512]{1,0:T(8,128)(2,1)} async-done(((bf16[768,2048]{1,0:T(8,128)(2,1)}), bf16[768,512]{1,0:T(8,128)(2,1)}) %reduce-scatter.4.cloned.1.call-update) | async-done | bytes 786448 | tf_op jit(solution)/shard_map/reduce_scatter | solution.py:86
  282.7 5.9 psum.22
  294.9 8.3 %multiply_cosine_fusion = (f32[2,128,256]{1,0,2:T(2,128)S(1)}, f32[2,128,256]{1,0,2:T(2,128)}, f32[2,128,256]{1,0,2:T(2,128)}) fusion(f32[2,128]{1,0:T(2,128)S(1)} %multiply_add_fusion.1, f32[256]{0:T(256)S(1)} %mul.404), kind=kLoop, calls=%fused_computation.82 | loop fusion | flops 327680 | bytes 788480 | tf_op jit(solution)/shard_map/cos | solution.py:35
  303.2 29.0 %all-gather.26.cloned.1.call-done = bf16[2048,512]{1,0:T(8,128)(2,1)} async-done(((bf16[256,512]{1,0:T(8,128)(2,1)}), bf16[2048,512]{1,0:T(8,128)(2,1)}) %all-gather.26.cloned.1.call-update) | async-done | bytes 2097168 | tf_op jit(solution)/shard_map/all_gather | solution.py:152
  332.2 28.6 %all-gather.20.cloned.1.call-done = bf16[768,2048]{1,0:T(8,128)(2,1)} async-done(((bf16[768,512]{1,0:T(8,128)(2,1)}), bf16[768,2048]{1,0:T(8,128)(2,1)}) %all-gather.20.cloned.1.call-update) | async-done | bytes 3145744 | tf_op jit(solution)/shard_map/all_gather | solution.py:81
  360.9 4.3 fusion.50
  369.1 43.0 %all-gather.22.cloned.1.call-done = bf16[2048,512]{1,0:T(8,128)(2,1)} async-done(((bf16[256,512]{1,0:T(8,128)(2,1)}), bf16[2048,512]{1,0:T(8,128)(2,1)}) %all-gather.22.cloned.1.call-update) | async-done | bytes 2097168 | tf_op jit(solution)/shard_map/all_gather | solution.py:153
  412.1 5.9 broadcast_multiply_fusion
  428.6 3.7 reshape_reshape.8
  436.1 4.1 reshape.160
  443.2 4.8 copy.58
  448.1 5.0 copy.62
  453.2 8.7 %all-gather.24.cloned.1.call-done = bf16[2048,512]{1,0:T(8,128)(2,1)} async-done(((bf16[256,512]{1,0:T(8,128)(2,1)}), bf16[2048,512]{1,0:T(8,128)(2,1)}) %all-gather.24.cloned.1.call-update) | async-done | bytes 2097168 | tf_op jit(solution)/shard_map/all_gather | solution.py:154
  461.9 5.6 fusion.49
  473.4 4.2 fusion.44
  477.7 32.1 %while.15 = (s32[]{:T(128)}, f32[3,2,256,256]{3,2,1,0:T(8,128)S(1)}, f32[2,3,128,2,256]{2,4,3,1,0:T(8,128)}, f32[2]{0:T(128)}, f32[2,3,128,2,256]{2,0,4,3,1:T(2,...) while((s32[]{:T(128)}, ...), condition=%wide.region_6.7_spmd.clone.clone.clone, body=%wide.region_5.6_spmd.clone.clone.clone.sunk | while | flops 1814266368 | bytes 24476680 | solution.py:69
  493.7 3.6 constant_dynamic-slice_fusion.3
  516.8 45.7 %all-gather.30.cloned.1.call-done = bf16[512,2048]{1,0:T(8,128)(2,1)} async-done(((bf16[512,256]{1,0:T(8,128)(2,1)}), bf16[512,2048]{1,0:T(8,128)(2,1)}) %all-gather.30.cloned.1.call-update) | async-done | bytes 2097168 | tf_op jit(solution)/shard_map/all_gather | solution.py:170
  562.5 9.0 %convolution_convert_fusion = bf16[768,2048]{1,0:T(8,128)(2,1)} fusion(bf16[512,2048]{1,0:T(8,128)(2,1)} %all-gather.30.cloned.1.call-done, f32[768,512]{1,0:T(8,128)} %bitcast.106, f32[768,512]{1,0:T(8,128)S(1)} %bitcast.105, bf16[768,2048]{1,0:T(8,128)(2,1)} %all-gather.20.cloned.1.call-done, bf16[2048,512]{1,0:T(8,128)(2,1)} %all-gather.28.cloned.1.call-done, ...), kind=kOutput, calls=%fused_computation.29 | convolution fusion | flops 3227123712 | bytes 13635584 | tf_op jit(solution)/shard_map/dot_general | solution.py:168
  571.5 36.0 %reduce-scatter.6.cloned.1.call-done = bf16[768,512]{1,0:T(8,128)(2,1)} async-done(((bf16[768,2048]{1,0:T(8,128)(2,1)}), bf16[768,512]{1,0:T(8,128)(2,1)}) %reduce-scatter.6.cloned.1.call-update) | async-done | bytes 786448 | tf_op jit(solution)/shard_map/reduce_scatter | solution.py:86
  609.0 5.8 psum.23
  616.1 29.2 %all-gather.32.cloned.1.call-done = bf16[768,2048]{1,0:T(8,128)(2,1)} async-done(((bf16[768,512]{1,0:T(8,128)(2,1)}), bf16[768,2048]{1,0:T(8,128)(2,1)}) %all-gather.32.cloned.1.call-update) | async-done | bytes 3145744 | tf_op jit(solution)/shard_map/all_gather | solution.py:81
  645.3 6.8 fusion.61
  652.1 11.8 %convolution_convert_fusion.1 = bf16[768,2048]{1,0:T(8,128)(2,1)} fusion(bf16[768,2048]{1,0:T(8,128)(2,1)} %all-gather.18.cloned.1.call-done, f32[768,768]{1,0:T(8,128)} %fusion.61, bf16[768,2048]{1,0:T(8,128)(2,1)} %all-gather.32.cloned.1.call-done, bf16[2048,768]{1,0:T(8,128)(2,1)} %all-gather.16.cloned.1.call-done, f32[768]{0:T(1024)S(1)} %copy-done.30, ...), kind=kOutput, calls=%fused_computation.30 | convolution fusion | flops 4838129664 | bytes 14948352 | tf_op jit(solution)/shard_map/dot_general | solution.py:103
  663.9 37.9 %reduce-scatter.8.cloned.1.call-done = bf16[768,512]{1,0:T(8,128)(2,1)} async-done(((bf16[768,2048]{1,0:T(8,128)(2,1)}), bf16[768,512]{1,0:T(8,128)(2,1)}) %reduce-scatter.8.cloned.1.call-update) | async-done | bytes 786448 | tf_op jit(solution)/shard_map/reduce_scatter | solution.py:86
  (189 shorter events, 83.7 us)
Async XLA Ops:
  6.5 12.2 %copy-start.8 = (f32[256,768]{1,0:T(8,128)S(1)}, f32[256,768]{1,0:T(8,128)}, u32[]{:S(2)}) copy-start(f32[256,768]{1,0:T(8,128)} %param.26) | copy-start | bytes 2359300
  6.5 41.1 %all-gather.12.cloned.1.call-start = ((), (), s32[]{:S(2)}) async-start(), calls=%async_computation.3 | async-start | bytes 3932160 | tf_op jit(solution)/shard_map/all_gather | solution.py:81
  18.7 91.2 %all-gather.14.cloned.1.call-start = ((), (), s32[]{:S(2)}) async-start(), calls=%async_computation.4 | async-start | bytes 3538944 | tf_op jit(solution)/shard_map/all_gather | solution.py:94
  19.5 151.2 %all-gather.16.cloned.1.call-start = ((), (), s32[]{:S(2)}) async-start(), calls=%async_computation.5 | async-start | bytes 3538944 | tf_op jit(solution)/shard_map/all_gather | solution.py:99
  20.7 213.3 %all-gather.18.cloned.1.call-start = ((), (), s32[]{:S(2)}) async-start(), calls=%async_computation.6 | async-start | bytes 3538944 | tf_op jit(solution)/shard_map/all_gather | solution.py:105
  21.6 212.4 %copy-start.29 = (f32[768]{0:T(1024)S(1)}, f32[768]{0:T(1024)}, u32[]{:S(2)}) copy-start(f32[768]{0:T(1024)} %param.30) | copy-start | bytes 9220
  21.6 212.4 %copy-start.31 = (f32[768]{0:T(1024)S(1)}, f32[768]{0:T(1024)}, u32[]{:S(2)}) copy-start(f32[768]{0:T(1024)} %param.29) | copy-start | bytes 9220
  21.6 259.5 %reduce-scatter.4.cloned.1.call-start = ((), (), s32[]{:S(2)}) async-start(), calls=%async_computation.7 | async-start | bytes 3932160 | tf_op jit(solution)/shard_map/reduce_scatter | solution.py:86
  47.6 186.4 %copy-start.28 = (bf16[768,2048]{1,0:T(8,128)(2,1)S(1)}, bf16[768,2048]{1,0:T(8,128)(2,1)}, u32[]{:S(2)}) copy-start(bf16[768,2048]{1,0:T(8,128)(2,1)} %all-gather.12.cloned.1.call-done) | copy-start | bytes 9437188
  245.0 36.1 %copy-start.1 = (bf16[768,512]{1,0:T(8,128)(2,1)S(1)}, bf16[768,512]{1,0:T(8,128)(2,1)}, u32[]{:S(2)}) copy-start(bf16[768,512]{1,0:T(8,128)(2,1)} %param.24) | copy-start | bytes 2359300
  245.1 43.5 %copy-start.24 = (f32[512]{0:T(512)S(1)}, f32[512]{0:T(512)}, u32[]{:S(2)}) copy-start(f32[512]{0:T(512)} %param.32) | copy-start | bytes 6148
  245.1 87.1 %all-gather.26.cloned.1.call-start = ((), (), s32[]{:S(2)}) async-start(), calls=%async_computation.11 | async-start | bytes 2359296 | tf_op jit(solution)/shard_map/all_gather | solution.py:152
  246.8 114.0 %all-gather.20.cloned.1.call-start = ((), (), s32[]{:S(2)}) async-start(), calls=%async_computation.8 | async-start | bytes 3932160 | tf_op jit(solution)/shard_map/all_gather | solution.py:81
  246.9 41.7 %copy-start.19 = (f32[512]{0:T(512)}, f32[512]{0:T(512)S(1)}, u32[]{:S(2)}) copy-start(f32[512]{0:T(512)S(1)} %broadcast_multiply_fusion.1) | copy-start | bytes 6148
  289.8 122.3 %all-gather.22.cloned.1.call-start = ((), (), s32[]{:S(2)}) async-start(), calls=%async_computation.9 | async-start | bytes 2359296 | tf_op jit(solution)/shard_map/all_gather | solution.py:153
  290.6 171.3 %all-gather.24.cloned.1.call-start = ((), (), s32[]{:S(2)}) async-start(), calls=%async_computation.10 | async-start | bytes 2359296 | tf_op jit(solution)/shard_map/all_gather | solution.py:154
  291.4 69.4 %copy-start.33 = (f32[512]{0:T(512)S(1)}, f32[512]{0:T(512)}, u32[]{:S(2)}) copy-start(f32[512]{0:T(512)} %param.37) | copy-start | bytes 6148
  291.5 225.3 %all-gather.28.cloned.1.call-start = ((), (), s32[]{:S(2)}) async-start(), calls=%async_computation.12 | async-start | bytes 2359296 | tf_op jit(solution)/shard_map/all_gather | solution.py:155
  292.3 270.2 %all-gather.30.cloned.1.call-start = ((), (), s32[]{:S(2)}) async-start(), calls=%async_computation.13 | async-start | bytes 2359296 | tf_op jit(solution)/shard_map/all_gather | solution.py:170
  293.1 314.4 %reduce-scatter.6.cloned.1.call-start = ((), (), s32[]{:S(2)}) async-start(), calls=%async_computation.14 | async-start | bytes 3932160 | tf_op jit(solution)/shard_map/reduce_scatter | solution.py:86
  366.9 45.2 %copy-start.34 = (f32[512]{0:T(512)S(1)}, f32[512]{0:T(512)}, u32[]{:S(2)}) copy-start(f32[512]{0:T(512)} %param.38) | copy-start | bytes 6148
  448.1 13.8 %copy-start.35 = (f32[512]{0:T(512)S(1)}, f32[512]{0:T(512)}, u32[]{:S(2)}) copy-start(f32[512]{0:T(512)} %param.39) | copy-start | bytes 6148
  515.5 47.0 %copy-start.36 = (f32[512]{0:T(512)S(1)}, f32[512]{0:T(512)}, u32[]{:S(2)}) copy-start(f32[512]{0:T(512)} %param.40) | copy-start | bytes 6148
  515.5 47.0 %copy-start.37 = (f32[512]{0:T(512)S(1)}, f32[512]{0:T(512)}, u32[]{:S(2)}) copy-start(f32[512]{0:T(512)} %param.41) | copy-start | bytes 6148
  571.4 36.1 %copy-start.3 = (bf16[768,512]{1,0:T(8,128)(2,1)S(1)}, bf16[768,512]{1,0:T(8,128)(2,1)}, u32[]{:S(2)}) copy-start(bf16[768,512]{1,0:T(8,128)(2,1)} %copy-done.2) | copy-start | bytes 2359300
  571.4 36.1 %copy-start.27 = (f32[512]{0:T(512)S(1)}, f32[512]{0:T(512)}, u32[]{:S(2)}) copy-start(f32[512]{0:T(512)} %param.44) | copy-start | bytes 6148
  571.5 43.4 %copy-start.25 = (f32[512]{0:T(512)S(1)}, f32[512]{0:T(512)}, u32[]{:S(2)}) copy-start(f32[512]{0:T(512)} %param.45) | copy-start | bytes 6148
  571.5 73.8 %all-gather.32.cloned.1.call-start = ((), (), s32[]{:S(2)}) async-start(), calls=%async_computation.15 | async-start | bytes 3932160 | tf_op jit(solution)/shard_map/all_gather | solution.py:81
  616.0 36.1 %copy-start.30 = (f32[768]{0:T(1024)S(1)}, f32[768]{0:T(1024)}, u32[]{:S(2)}) copy-start(f32[768]{0:T(1024)} %param.30) | copy-start | bytes 9220
  616.0 36.1 %copy-start.32 = (f32[768]{0:T(1024)S(1)}, f32[768]{0:T(1024)}, u32[]{:S(2)}) copy-start(f32[768]{0:T(1024)} %param.29) | copy-start | bytes 9220
  616.0 85.8 %reduce-scatter.8.cloned.1.call-start = ((), (), s32[]{:S(2)}) async-start(), calls=%async_computation.16 | async-start | bytes 3932160 | tf_op jit(solution)/shard_map/reduce_scatter | solution.py:86
  663.9 37.9 %copy-start.20 = (f32[512]{0:T(512)S(1)}, f32[512]{0:T(512)}, u32[]{:S(2)}) copy-start(f32[512]{0:T(512)} %copy-done.19) | copy-start | bytes 6148
  (30 other events, 79.6 us)
Sparse Core Ops, SparseCore 0:
  18.8 28.8 all-gather.11
  49.8 60.0 all-gather.13
  112.1 58.6 all-gather.15
  172.7 61.3 all-gather.17
  245.2 35.8 reduce-scatter.3
  283.1 49.0 all-gather.25
  333.8 27.0 all-gather.19
  363.0 49.0 all-gather.21
  414.2 47.6 all-gather.23
  463.9 47.6 all-gather.27
  513.6 48.8 all-gather.29
  571.6 35.8 reduce-scatter.5
  616.1 29.1 all-gather.31
  664.1 37.7 reduce-scatter.7
where the time goes:
time: 719 us; the launch traced here: 711 us
  waiting for transfers between devices  498 us (69%)
  matrix products  81.8 us (11%)
  local copies, waits for them, and re-layouts  52.9 us (7%)
  other arithmetic  43.2 us (6%)
  blocking collectives  20 us (3%)
  between operations  14.1 us (2%)
    reduce_scatter x3, waiting for transfers between devices, summed_share(): lax.psum_scatter(rounded.astype(jnp.float32).astype(jnp.bfloat16), 'tp',...  108 us
    all_gather x3, waiting for transfers between devices, normed_rows(): return lax.all_gather(scaled.astype(jnp.bfloat16), 'tp', axis=1, tiled=True)  83.8 us
    all_gather x1, waiting for transfers between devices, ffn_gathered(): lax.all_gather(down_low, 'fs', axis=1, tiled=True)  63.2 us
    all_gather x1, waiting for transfers between devices, ffn_gathered(): lax.all_gather(gate_low, 'fs', axis=0, tiled=True)  62.2 us
    all_gather x1, waiting for transfers between devices, ffn_gathered(): lax.all_gather(up_low, 'fs', axis=0, tiled=True)  54 us
    all_gather x1, waiting for transfers between devices, per_device(): lax.all_gather(w_mix.astype(jnp.bfloat16), 'fs', axis=1, tiled=True)  45.7 us
    all_gather x1, waiting for transfers between devices, per_device(): lax.all_gather(w_key.astype(jnp.bfloat16), 'fs', axis=0, tiled=True)  43 us
    all_gather x1, waiting for transfers between devices, per_device(): lax.all_gather(w_query.astype(jnp.bfloat16), 'fs', axis=0, tiled=True)  29 us
  transfers between devices with their start and end apart: 14, of which 13 were waited for; matrix products, arithmetic and copies ran while one was open for 18% of the time, Pallas kernels for 0%

commit v1 on v0

v1 whole, which is shorter than its diff:
```python
import functools

import jax
import jax.numpy as jnp
import numpy as np
from jax import lax
from jax.experimental import pallas as pl
from jax.experimental.pallas import tpu as pltpu
from jax.sharding import PartitionSpec as P

LEN = 256
EPS = 1e-06
HEAD_EPS = 0.1
MESH = pl.DeviceIdType.MESH
BF16 = jnp.bfloat16
F32 = jnp.float32


def rows_of(ref, piece, rows):
    return ref.at[pl.ds(piece * rows, rows)]


def cols_at(index, width):
    return pl.ds(pl.multiple_of(index * width, width), width)


def remote(src, dst, send_sem, recv_sem, axis, target):
    return pltpu.make_async_remote_copy(
        src_ref=src,
        dst_ref=dst,
        send_sem=send_sem,
        recv_sem=recv_sem,
        device_id={axis: target},
        device_id_type=MESH,
    )


class TpGather:
    def __init__(self, ntp, src, out, sends, forwards, recvs, pieces):
        self.t = lax.axis_index("tp")
        self.nx = ntp // 2
        self.core = lax.rem(self.t, 2)
        self.chip = lax.div(self.t, 2)
        self.partner = self.chip * 2 + (1 - self.core)
        self.src, self.out = src, out
        self.sends, self.forwards, self.recvs = sends, forwards, recvs
        self.pieces = pieces
        self.rows = src.shape[0] // pieces
        self.width = src.shape[1]

    def along_x(self, offset, core):
        return lax.rem(self.chip + offset, self.nx) * 2 + core

    def place(self, index, piece):
        return self.out.at[pl.ds(piece * self.rows, self.rows), cols_at(index, self.width)]

    def own_sends(self, piece):
        src = rows_of(self.src, piece, self.rows)
        copies = []
        for offset in range(self.nx - 1, -1, -1):
            target = self.along_x(offset, self.core) if offset else self.partner
            copies.append(
                remote(
                    src,
                    self.place(self.t, piece),
                    self.sends.at[offset, piece],
                    self.recvs.at[self.t, piece],
                    "tp",
                    target,
                )
            )
        return copies

    def forward(self, offset, piece):
        index = self.along_x(self.nx - offset, self.core)
        block = self.place(index, piece)
        return remote(
            block,
            block,
            self.forwards.at[offset, piece],
            self.recvs.at[index, piece],
            "tp",
            self.partner,
        )

    def arrived(self, index, piece):
        block = self.place(index, piece)
        remote(
            block,
            block,
            self.sends.at[0, piece],
            self.recvs.at[index, piece],
            "tp",
            self.partner,
        ).wait_recv()

    def start(self, piece):
        for copy in self.own_sends(piece):
            copy.start()

    def relay(self):
        for piece in range(self.pieces):
            for offset in range(1, self.nx):
                self.arrived(self.along_x(self.nx - offset, self.core), piece)
                self.forward(offset, piece).start()

    def finish(self):
        for piece in range(self.pieces):
            for offset in range(self.nx):
                self.arrived(self.along_x(offset, 1 - self.core), piece)
        for piece in range(self.pieces):
            for copy in self.own_sends(piece):
                copy.wait_send()
            for offset in range(1, self.nx):
                self.forward(offset, piece).wait_send()


def greet_tp(ntp, barrier):
    t = lax.axis_index("tp")
    for offset in range(1, ntp):
        pl.semaphore_signal(
            barrier, inc=1, device_id={"tp": lax.rem(t + offset, ntp)}, device_id_type=MESH
        )


def entry_kernel(
    nfs, ntp, ny, pieces,
    gate, up, down, tok, gains,
    gate_out, up_out, down_out, tok_out, gains_out,
    own_sem, send_sem, recv_sem, tok_own, tok_send, tok_fwd, tok_recv,
    gain_own, gain_send, gain_fwd, gain_recv,
):
    nz = nfs // ny
    f = lax.axis_index("fs")
    z, y = lax.div(f, ny), lax.rem(f, ny)
    barrier = pltpu.get_barrier_semaphore()
    greet_tp(ntp, barrier)
    for offset in range(1, ny):
        other = z * ny + lax.rem(y + offset, ny)
        pl.semaphore_signal(barrier, inc=1, device_id={"fs": other}, device_id_type=MESH)

    @pl.when(z > 0)
    def _():
        pl.semaphore_signal(barrier, inc=1, device_id={"fs": f - ny}, device_id_type=MESH)

    @pl.when(z < nz - 1)
    def _():
        pl.semaphore_signal(barrier, inc=1, device_id={"fs": f + ny}, device_id_type=MESH)

    ends = (z > 0).astype(jnp.int32) + (z < nz - 1).astype(jnp.int32)
    pl.semaphore_wait(barrier, ntp + ny - 2 + ends)

    shards = (gate, up, down)
    outs = (gate_out, up_out, down_out)

    def place(p, index):
        if p < 2:
            return outs[p].at[cols_at(index, shards[p].shape[0])]
        return outs[p].at[:, cols_at(index, shards[p].shape[1])]

    def along_z(p, step, zs, own):
        index = zs * ny + y
        block = place(p, index)
        kind = 0 if step > 0 else 1
        return remote(
            shards[p] if own else block, block, send_sem.at[kind, zs, p],
            recv_sem.at[index, p], "fs", f + step * ny,
        )

    def along_y(p, offset, zs, own):
        index = zs * ny + y
        block = place(p, index)
        return remote(
            shards[p] if own else block, block, send_sem.at[1 + offset, zs, p],
            recv_sem.at[index, p], "fs", z * ny + lax.rem(y + offset, ny),
        )

    def arrived(p, index):
        block = place(p, index)
        remote(block, block, send_sem.at[0, 0, p], recv_sem.at[index, p], "fs", f).wait_recv()

    toks = TpGather(ntp, tok, tok_out, tok_send, tok_fwd, tok_recv, pieces)
    gain = TpGather(ntp, gains, gains_out, gain_send, gain_fwd, gain_recv, 1)
    locals_ = [
        pltpu.make_async_copy(shards[p], place(p, f), own_sem.at[p]) for p in range(3)
    ]
    locals_.append(pltpu.make_async_copy(tok, tok_out.at[:, cols_at(toks.t, toks.width)], tok_own))
    locals_.append(
        pltpu.make_async_copy(gains, gains_out.at[:, cols_at(gain.t, gain.width)], gain_own)
    )

    def sends(zs, p, source_step, own, act):
        for step in (1, -1):
            if own or step == source_step:
                inside = (z < nz - 1) if step > 0 else (z > 0)

                @pl.when(inside)
                def _():
                    act(along_z(p, step, zs, own))

        for offset in range(1, ny):
            act(along_y(p, offset, zs, own))

    def all_z(act, wait):
        for distance in range(1, nz):
            for p in range(3):
                for step in (1, -1):
                    zs = z - step * distance

                    @pl.when(jnp.logical_and(zs >= 0, zs < nz))
                    def _():
                        if wait:
                            arrived(p, zs * ny + y)
                        sends(zs, p, step, False, act)

    for p in range(3):
        sends(z, p, 0, True, lambda copy: copy.start())
    gain.start(0)
    for piece in range(pieces):
        toks.start(piece)
    for copy in locals_:
        copy.start()
    gain.relay()
    toks.relay()
    all_z(lambda copy: copy.start(), True)
    for copy in locals_:
        copy.wait()
    gain.finish()
    toks.finish()
    for zs in range(nz):
        for p in range(3):
            for offset in range(1, ny):
                arrived(p, zs * ny + lax.rem(y + offset, ny))
    for p in range(3):
        sends(z, p, 0, True, lambda copy: copy.wait_send())
    all_z(lambda copy: copy.wait_send(), False)


def reduce_kernel(
    ntp, pieces, factor, gather,
    part, res, scale, *refs,
):
    if gather:
        (out, full, one, pair, two, s1, v1, s2, v2, own_sem, g_send, g_fwd, g_recv) = refs
    else:
        (out, one, pair, two, s1, v1, s2, v2) = refs
    t = lax.axis_index("tp")
    nx = ntp // 2
    core, chip = lax.rem(t, 2), lax.div(t, 2)
    partner = chip * 2 + (1 - core)
    width = res.shape[1]
    rows = res.shape[0] // pieces

    def at(piece):
        return pl.ds(piece * rows, rows)

    def along_x(offset, which):
        return lax.rem(chip + offset, nx) * 2 + which

    def to_partner(offset, piece):
        return remote(
            part.at[at(piece), cols_at(along_x(offset, 1 - core), width)],
            one.at[offset, at(piece)],
            s1.at[offset, piece], v1.at[offset, piece], "tp", partner,
        )

    def across(offset, piece):
        return remote(
            pair.at[offset - 1, at(piece)],
            two.at[offset - 1, at(piece)],
            s2.at[offset - 1, piece], v2.at[offset - 1, piece], "tp", along_x(offset, core),
        )

    barrier = pltpu.get_barrier_semaphore()
    greet_tp(ntp, barrier)
    pl.semaphore_wait(barrier, ntp - 1)
    for piece in range(pieces):
        for offset in range(1, nx):
            to_partner(offset, piece).start()
    for piece in range(pieces):
        to_partner(0, piece).start()
    for piece in range(pieces):
        for offset in range(1, nx):
            to_partner(offset, piece).wait_recv()
            mine = part[at(piece), cols_at(along_x(offset, core), width)].astype(F32)
            total = mine + one[offset, at(piece)].astype(F32)
            pair[offset - 1, at(piece)] = total.astype(BF16)
            across(offset, piece).start()
    if gather:
        spread = TpGather(ntp, out, full, g_send, g_fwd, g_recv, pieces)
    for piece in range(pieces):
        to_partner(0, piece).wait_recv()
        total = part[at(piece), cols_at(t, width)].astype(F32) + one[0, at(piece)].astype(F32)
        for offset in range(1, nx):
            across(offset, piece).wait_recv()
            total = total + two[offset - 1, at(piece)].astype(F32)
        value = res[at(piece)].astype(F32) + factor * total * scale[...]
        out[at(piece)] = value.astype(BF16)
        if gather:
            spread.start(piece)
    if gather:
        own = pltpu.make_async_copy(out, full.at[:, cols_at(t, width)], own_sem)
        own.start()
        spread.relay()
        spread.finish()
        own.wait()
    for piece in range(pieces):
        for offset in range(nx):
            to_partner(offset, piece).wait_send()
        for offset in range(1, nx):
            across(offset, piece).wait_send()


def retain_kernel(rate, query, key, value, outgate, cosines, sines, gain, out):
    length, width = query.shape
    even = lax.rem(lax.broadcasted_iota(jnp.int32, (length, width), 1), 2) == 0

    def turned(ref):
        v = ref[...].astype(F32)
        swapped = jnp.where(even, -pltpu.roll(v, width - 1, 1), pltpu.roll(v, 1, 1))
        return v * cosines[...] + swapped * sines[...]

    q = turned(query).astype(BF16)
    k = (turned(key) * width ** -0.5).astype(BF16)
    scores = lax.dot_general(q, k, (((1,), (1,)), ((), ())), preferred_element_type=F32)
    distance = lax.broadcasted_iota(jnp.int32, (length, length), 0) - lax.broadcasted_iota(
        jnp.int32, (length, length), 1
    )
    decay = jnp.exp(-rate[pl.program_id(0), 0] * jnp.maximum(distance, 0).astype(F32))
    scores = jnp.where(distance >= 0, scores * decay, 0.0).astype(BF16)
    kept = jnp.dot(scores, value[...], preferred_element_type=F32)
    kept = kept * lax.rsqrt(jnp.mean(kept * kept, axis=1, keepdims=True) + HEAD_EPS)
    g = outgate[...].astype(F32)
    out[...] = (kept * gain[...] * (g / (1.0 + jnp.exp(-g)))).astype(BF16)


def vmem():
    return pl.BlockSpec(memory_space=pltpu.VMEM)


def anywhere():
    return pl.BlockSpec(memory_space=pl.ANY)


def dma(*shape):
    return pltpu.SemaphoreType.DMA(shape)


def cost(flops):
    return pl.CostEstimate(flops=flops, bytes_accessed=2**20, transcendentals=0)


def enter(nfs, ntp, gate, up, down, tok, gains):
    ny = ntp // 2 if nfs % (ntp // 2) == 0 else 1
    nz, nx = nfs // ny, ntp // 2
    pieces = tok.shape[0] // LEN
    shape = jax.ShapeDtypeStruct
    return pl.pallas_call(
        functools.partial(entry_kernel, nfs, ntp, ny, pieces),
        out_shape=(
            shape((gate.shape[0] * nfs, gate.shape[1]), BF16),
            shape((up.shape[0] * nfs, up.shape[1]), BF16),
            shape((down.shape[0], down.shape[1] * nfs), BF16),
            shape((tok.shape[0], tok.shape[1] * ntp), BF16),
            shape((gains.shape[0], gains.shape[1] * ntp), F32),
        ),
        in_specs=[vmem()] * 5,
        out_specs=(anywhere(),) * 5,
        scratch_shapes=[
            dma(3), dma(ny + 1, nz, 3), dma(nfs, 3),
            dma(), dma(nx, pieces), dma(nx, pieces), dma(ntp, pieces),
            dma(), dma(nx, 1), dma(nx, 1), dma(ntp, 1),
        ],
        compiler_params=pltpu.CompilerParams(collective_id=0, has_side_effects=True),
        cost_estimate=cost(10**11),
        name="enter",
    )(gate, up, down, tok, gains)


def combine(ntp, identity, factor, gather, part, res, scale):
    pieces = res.shape[0] // LEN
    nx = ntp // 2
    rows, width = res.shape
    shape = jax.ShapeDtypeStruct
    out_shape = [shape((rows, width), BF16)]
    out_specs = [vmem()]
    scratch = [
        pltpu.VMEM((nx, rows, width), BF16),
        pltpu.VMEM((max(nx - 1, 1), rows, width), BF16),
        pltpu.VMEM((max(nx - 1, 1), rows, width), BF16),
        dma(nx, pieces), dma(nx, pieces),
        dma(max(nx - 1, 1), pieces), dma(max(nx - 1, 1), pieces),
    ]
    if gather:
        out_shape.append(shape((rows, width * ntp), BF16))
        out_specs.append(anywhere())
        scratch += [dma(), dma(nx, pieces), dma(nx, pieces), dma(ntp, pieces)]
    return pl.pallas_call(
        functools.partial(reduce_kernel, ntp, pieces, factor, gather),
        out_shape=tuple(out_shape),
        in_specs=[vmem()] * 3,
        out_specs=tuple(out_specs),
        scratch_shapes=scratch,
        compiler_params=pltpu.CompilerParams(collective_id=identity, has_side_effects=True),
        cost_estimate=cost(4 * 10**10),
        name="combine",
    )(part, res, scale)


def tables(length, width):
    freq = np.float32(1.0) / np.float32(10000.0) ** np.linspace(0.0, 1.0, width // 2, dtype=np.float32)
    angles = np.arange(length, dtype=np.float32)[:, None] * np.repeat(freq, 2)[None, :]
    return jnp.asarray(np.cos(angles)), jnp.asarray(np.sin(angles))


def retain(query, key, value, outgate, decay_rate, ret_gain):
    heads = decay_rate.shape[0]
    width = query.shape[1] // heads
    cosines, sines = tables(LEN, width)
    block = pl.BlockSpec((LEN, width), lambda h, s: (s, h))
    whole = pl.BlockSpec((LEN, width), lambda h, s: (0, 0))
    return pl.pallas_call(
        retain_kernel,
        grid=(heads, query.shape[0] // LEN),
        out_shape=jax.ShapeDtypeStruct(query.shape, BF16),
        in_specs=[
            pl.BlockSpec(memory_space=pltpu.SMEM), block, block, block, block, whole, whole,
            pl.BlockSpec((1, width), lambda h, s: (0, h)),
        ],
        out_specs=block,
        cost_estimate=cost(10**10),
        name="retain",
    )(decay_rate[:, None], query, key, value, outgate, cosines, sines, ret_gain[None])


def normed(full, gain):
    widened = full.astype(F32)
    mean = jnp.mean(widened * widened, axis=1, keepdims=True)
    return (widened * lax.rsqrt(mean + EPS) * gain).astype(BF16)


def dot(left, right):
    return jnp.dot(left, right, preferred_element_type=F32)


def ffn_part(features, gate, up, down, scale_gate, scale_up):
    hidden = jax.nn.silu(dot(features, gate) * scale_gate) * (dot(features, up) * scale_up)
    return dot(hidden.astype(BF16), down).astype(BF16)


def per_device(
    nfs, ntp,
    tokens, gain_one, w_gate, w_up, w_down, scale_gate, scale_up, scale_down,
    gain_mix, w_query, w_key, w_value, w_outgate,
    scale_query, scale_key, scale_value, scale_outgate,
    ret_gain, decay_rate, w_mix, scale_mix, gain_two,
):
    def gathered(weight, axis):
        return lax.all_gather(weight.astype(BF16), "fs", axis=axis, tiled=True)

    weights = [gathered(w, 0) for w in (w_query, w_key, w_value, w_outgate)]
    mix = gathered(w_mix, 1)
    gains = jnp.pad(jnp.stack((gain_one, gain_mix, gain_two)), ((0, 5), (0, 0)))
    gate, up, down, full, gains = enter(
        nfs, ntp, w_gate.astype(BF16), w_up.astype(BF16), w_down.astype(BF16), tokens, gains
    )
    part = ffn_part(normed(full, gains[0]), gate, up, down, scale_gate, scale_up)
    first, full = combine(ntp, 1, 0.5, True, part, tokens, scale_down[None])
    features = normed(full, gains[1])
    scales = (scale_query, scale_key, scale_value, scale_outgate)
    rows = [(dot(features, w) * s).astype(BF16) for w, s in zip(weights, scales)]
    mixed = retain(*rows, decay_rate, ret_gain)
    part = dot(mixed, mix).astype(BF16)
    second, full = combine(ntp, 2, 1.0, True, part, first, scale_mix[None])
    part = ffn_part(normed(full, gains[2]), gate, up, down, scale_gate, scale_up)
    return combine(ntp, 3, 0.5, False, part, second, scale_down[None])[0]


def solution(mesh):
    return jax.shard_map(
        functools.partial(per_device, mesh.shape["fs"], mesh.shape["tp"]),
        mesh=mesh,
        in_specs=(
            P("fs", "tp"),
            P("tp"),
            P("fs", "tp"),
            P("fs", "tp"),
            P("tp", "fs"),
            P("tp"),
            P("tp"),
            P("tp"),
            P("tp"),
            P("fs", "tp"),
            P("fs", "tp"),
            P("fs", "tp"),
            P("fs", "tp"),
            P("tp"),
            P("tp"),
            P("tp"),
            P("tp"),
            P("tp"),
            P("tp"),
            P("tp", "fs"),
            P("tp"),
            P("tp"),
        ),
        out_specs=P("fs", "tp"),
        check_vma=False,
    )
```

time: 719 us -> 402 us (0.56)
  waiting for transfers between devices: 498 us -> 46.1 us
  Pallas kernels: 0 us -> 262 us
  local copies, waits for them, and re-layouts: 52.9 us -> 4.01 us
  other arithmetic: 43.2 us -> 18.1 us
  matrix products: 81.8 us -> 57 us
  blocking collectives: 20 us -> 0 us
    all_gather x11 -> x5, waiting for transfers between devices: 390 us -> 46 us  [gathered(): return lax.all_gather(weight.astype(BF16), 'fs', axis=axis, tiled=True)]
    pallas_call x0 -> x5, Pallas kernels: none -> 262 us  [the longest x1 145 us: enter(): pl.pallas_call(functools.partial(entry_kernel, nfs, ntp, ny, pieces), out...]
    reduce_scatter x3 -> x0, waiting for transfers between devices: 108 us -> none  [summed_share(): lax.psum_scatter(rounded.astype(jnp.float32).astype(jnp.bfloat16), 'tp',...]
    dot_general x16 -> x9, matrix products: 81.8 us -> 57 us  [dot(): return jnp.dot(left, right, preferred_element_type=F32)]
    reshape x6 -> x0, local copies, waits for them, and re-layouts: 22.3 us -> none  [the longest x4 15.1 us: split_heads(): values.astype(jnp.float32).reshape(sequences, length, heads, head_size)]
    psum x3 -> x0, blocking collectives: 20 us -> none  [normed_rows(): totals = lax.psum(jnp.sum(widened * widened, axis=1), 'tp')]
    transpose x3 -> x0, local copies, waits for them, and re-layouts: 8.81 us -> none  [the longest x2 5.98 us: to_blocks(): jnp.moveaxis(values.reshape(sequences, nblocks, block, heads, head_size),...]
    cos x1 -> x0, other arithmetic: 8.35 us -> none  [retain(): cosines = jnp.cos(angles)[None, :, None, :]]
  transfers between devices with their start and end apart: 14 -> 5, of which waited for: 13 -> 2; matrix products, arithmetic and copies ran while one was open for 18% -> 12% of each run, Pallas kernels for 0% -> 48%
where the time goes in v1:
time: 402 us; the launch traced here: 401 us
  Pallas kernels  262 us (65%)
  matrix products  57 us (14%)
  waiting for transfers between devices  46.1 us (11%)
  other arithmetic  18.1 us (5%)
  between operations  13.3 us (3%)
    pallas_call x1, Pallas kernels, enter(): pl.pallas_call(functools.partial(entry_kernel, nfs, ntp, ny, pieces), out...  145 us
    pallas_call x3, Pallas kernels, combine(): pl.pallas_call(functools.partial(reduce_kernel, ntp, pieces, factor, gath...  111 us
    dot_general x9, matrix products, dot(): return jnp.dot(left, right, preferred_element_type=F32)  57 us
    all_gather x5, waiting for transfers between devices, gathered(): return lax.all_gather(weight.astype(BF16), 'fs', axis=axis, tiled=True)  46 us
  transfers between devices with their start and end apart: 5, of which 2 were waited for; matrix products, arithmetic and copies ran while one was open for 12% of the time, Pallas kernels for 48%

profile of v1, /device:TPU:0, one launch (start us, length us, event | category | flops | bytes accessed | tf_op | source)
XLA Modules:
  0.0 401.2 jit_solution(18141049801272731513)
XLA Ops:
  6.6 1.9 convert_element_type.86
  8.6 1.8 convert_element_type.84
  10.5 1.8 convert_element_type.82
  12.4 0.7 convert_element_type.80
  13.2 0.8 convert_element_type.88
  14.0 0.8 convert_element_type.71.gate
  14.8 0.8 convert_element_type.72.up
  15.6 0.8 convert_element_type.73.down
  16.4 0.6 select_maximum_fusion.gains
  17.0 144.6 %enter.1 = (bf16[2048,768]{1,0:T(8,128)(2,1)}, bf16[2048,768]{1,0:T(8,128)(2,1)}, bf16[768,2048]{1,0:T(8,128)(2,1)}, bf16[768,2048]{1,0:T(8,128)(2,1)}, f32[8,2048]{1,0:T(8,128)}) custom-call(bf16[256,768]{1,0:T(8,128)(2,1)} %convert_element_type.71.gate, bf16[256,768]{1,0:T(8,128)(2,1)} %convert_element_type.72.up, ...), custom_call_target="tpu_custom_call" | custom-call | flops 99999997952 | bytes 1048576 | tf_op jit(solution)/shard_map/enter/pallas_call | solution.py:358
  161.6 1.1 fusion.25
  162.7 2.6 fusion
  165.3 0.6 copy.25.rate
  165.9 6.0 %fusion.15 = f32[768,768]{1,0:T(8,128)} fusion(bf16[2048,768]{1,0:T(8,128)(2,1)} %get-tuple-element.16, bf16[768,2048]{1,0:T(8,128)(2,1)S(1)} %copy-done.1, f32[2048]{0:T(1024)S(1)} %bitcast.28, f32[768]{0:T(1024)S(1)} %add_rsqrt_fusion.2), kind=kOutput, calls=%fused_computation.25 | convolution fusion | flops 2422210560 | bytes 8662016 | tf_op jit(solution)/shard_map/dot_general | solution.py:443
  171.9 11.1 %convolution_convert_fusion.2.part = bf16[768,2048]{1,0:T(8,128)(2,1)} fusion(bf16[768,2048]{1,0:T(8,128)(2,1)} %get-tuple-element.18, f32[768,768]{1,0:T(8,128)} %fusion.15, bf16[2048,768]{1,0:T(8,128)(2,1)} %get-tuple-element.17, f32[768]{0:T(1024)S(1)} %copy-done.11, f32[768]{0:T(1024)S(1)} %copy-done.12, bf16[768,2048]{1,0:T(8,128)(2,1)S(1)} %copy-done.1, ...), kind=kOutput, calls=%fused_computation.17 | convolution fusion | flops 4844421120 | bytes 14959616 | tf_op jit(solution)/shard_map/dot_general | solution.py:443
  183.0 43.2 %combine.3 = (bf16[768,512]{1,0:T(8,128)(2,1)}, bf16[768,2048]{1,0:T(8,128)(2,1)}) custom-call(bf16[768,2048]{1,0:T(8,128)(2,1)} %convolution_convert_fusion.2.part, bf16[768,512]{1,0:T(8,128)(2,1)} %res.1, f32[1,512]{1,0:T(1,128)} %bitcast.35), custom_call_target="tpu_custom_call" | custom-call | flops 40000000000 | bytes 1048576 | tf_op jit(solution)/shard_map/combine/pallas_call | solution.py:398
  226.2 2.7 fusion.3
  229.0 0.1 copy-done
  229.1 4.3 %multiply_convert_fusion.2.outgate = bf16[768,512]{1,0:T(8,128)(2,1)} fusion(bf16[2048,512]{1,0:T(8,128)(2,1)} %all-gather.12.cloned.1.call-done, f32[512]{0:T(512)S(1)} %copy-done.13, bf16[768,2048]{1,0:T(8,128)(2,1)S(1)} %copy-done, f32[2048]{0:T(1024)S(1)} %bitcast.24, f32[768]{0:T(1024)S(1)} %add_rsqrt_fusion.1), kind=kOutput, calls=%fused_computation.20 | convolution fusion | flops 1617690624 | bytes 6042624 | tf_op jit(solution)/shard_map/dot_general | solution.py:443
  233.4 4.6 %multiply_convert_fusion.3.value = bf16[768,512]{1,0:T(8,128)(2,1)} fusion(bf16[2048,512]{1,0:T(8,128)(2,1)} %all-gather.10.cloned.1.call-done, f32[512]{0:T(512)S(1)} %copy-done.14, bf16[768,2048]{1,0:T(8,128)(2,1)S(1)} %copy-done, f32[2048]{0:T(1024)S(1)} %bitcast.25, f32[768]{0:T(1024)S(1)} %add_rsqrt_fusion.1), kind=kOutput, calls=%fused_computation.21 | convolution fusion | flops 1617690624 | bytes 6042624 | tf_op jit(solution)/shard_map/dot_general | solution.py:443
  238.0 4.4 %multiply_convert_fusion.4.key = bf16[768,512]{1,0:T(8,128)(2,1)} fusion(bf16[2048,512]{1,0:T(8,128)(2,1)} %all-gather.8.cloned.1.call-done, f32[512]{0:T(512)S(1)} %copy-done.15, bf16[768,2048]{1,0:T(8,128)(2,1)S(1)} %copy-done, f32[2048]{0:T(1024)S(1)} %bitcast.26, f32[768]{0:T(1024)S(1)} %add_rsqrt_fusion.1), kind=kOutput, calls=%fused_computation.22 | convolution fusion | flops 1617690624 | bytes 6042624 | tf_op jit(solution)/shard_map/dot_general | solution.py:443
  242.4 6.4 %all-gather.6.cloned.1.call-done = bf16[2048,512]{1,0:T(8,128)(2,1)} async-done(((bf16[256,512]{1,0:T(8,128)(2,1)}), bf16[2048,512]{1,0:T(8,128)(2,1)}) %all-gather.6.cloned.1.call-update) | async-done | bytes 2097168 | tf_op jit(solution)/shard_map/all_gather | solution.py:459
  248.8 4.3 %multiply_convert_fusion.5.query = bf16[768,512]{1,0:T(8,128)(2,1)} fusion(bf16[2048,512]{1,0:T(8,128)(2,1)} %all-gather.6.cloned.1.call-done, f32[512]{0:T(512)S(1)} %copy-done.16, bf16[768,2048]{1,0:T(8,128)(2,1)S(1)} %copy-done, f32[2048]{0:T(1024)S(1)} %bitcast.27, f32[768]{0:T(1024)S(1)} %add_rsqrt_fusion.1), kind=kOutput, calls=%fused_computation.23 | convolution fusion | flops 1617690624 | bytes 6042624 | tf_op jit(solution)/shard_map/dot_general | solution.py:443
  253.1 6.8 %retain.1 = bf16[768,512]{1,0:T(8,128)(2,1)} custom-call(f32[2,1]{1,0:T(2,128)} %copy.25.rate, bf16[768,512]{1,0:T(8,128)(2,1)} %multiply_convert_fusion.5.query, bf16[768,512]{1,0:T(8,128)(2,1)} %multiply_convert_fusion.4.key, bf16[768,512]{1,0:T(8,128)(2,1)} %multiply_convert_fusion.3.value, bf16[768,512]{1,0:T(8,128)(2,1)} %multiply_convert_fusion.2.outgate, ...), custom_call_target="tpu_custom_call" | custom-call | flops 10000000000 | bytes 1048576 | tf_op jit(solution)/shard_map/retain/pallas_call | solution.py:422
  259.9 39.6 %all-gather.14.cloned.1.call-done = bf16[512,2048]{1,0:T(8,128)(2,1)} async-done(((bf16[512,256]{1,0:T(8,128)(2,1)}), bf16[512,2048]{1,0:T(8,128)(2,1)}) %all-gather.14.cloned.1.call-update) | async-done | bytes 2097168 | tf_op jit(solution)/shard_map/all_gather | solution.py:459
  299.5 5.3 %convolution_convert_fusion.part = bf16[768,2048]{1,0:T(8,128)(2,1)} fusion(bf16[768,512]{1,0:T(8,128)(2,1)} %retain.1, bf16[512,2048]{1,0:T(8,128)(2,1)} %all-gather.14.cloned.1.call-done), kind=kOutput, calls=%fused_computation.15 | convolution fusion | flops 1612185600 | bytes 6029312 | tf_op jit(solution)/shard_map/dot_general | solution.py:443
  304.8 43.2 %combine.4 = (bf16[768,512]{1,0:T(8,128)(2,1)}, bf16[768,2048]{1,0:T(8,128)(2,1)}) custom-call(bf16[768,2048]{1,0:T(8,128)(2,1)} %convolution_convert_fusion.part, bf16[768,512]{1,0:T(8,128)(2,1)} %get-tuple-element.20.res, f32[1,512]{1,0:T(1,128)} %bitcast.34), custom_call_target="tpu_custom_call" | custom-call | flops 40000000000 | bytes 1048576 | tf_op jit(solution)/shard_map/combine/pallas_call | solution.py:398
  348.1 2.7 fusion.6
  350.9 5.9 %fusion.10 = f32[768,768]{1,0:T(8,128)} fusion(bf16[2048,768]{1,0:T(8,128)(2,1)} %get-tuple-element.16, bf16[768,2048]{1,0:T(8,128)(2,1)S(1)} %copy-done.2, f32[2048]{0:T(1024)S(1)} %bitcast.22, f32[768]{0:T(1024)S(1)} %add_rsqrt_fusion), kind=kOutput, calls=%fused_computation.24 | convolution fusion | flops 2422210560 | bytes 8662016 | tf_op jit(solution)/shard_map/dot_general | solution.py:443
  356.9 11.1 %convolution_convert_fusion.1.part = bf16[768,2048]{1,0:T(8,128)(2,1)} fusion(bf16[768,2048]{1,0:T(8,128)(2,1)} %get-tuple-element.18, f32[768,768]{1,0:T(8,128)} %fusion.10, bf16[2048,768]{1,0:T(8,128)(2,1)} %get-tuple-element.17, f32[768]{0:T(1024)S(1)} %copy-done.11, f32[768]{0:T(1024)S(1)} %copy-done.12, bf16[768,2048]{1,0:T(8,128)(2,1)S(1)} %copy-done.2, ...), kind=kOutput, calls=%fused_computation.16 | convolution fusion | flops 4844421120 | bytes 14959616 | tf_op jit(solution)/shard_map/dot_general | solution.py:443
  368.0 24.7 %combine.5 = bf16[768,512]{1,0:T(8,128)(2,1)} custom-call(bf16[768,2048]{1,0:T(8,128)(2,1)} %convolution_convert_fusion.1.part, bf16[768,512]{1,0:T(8,128)(2,1)} %get-tuple-element.22.res, f32[1,512]{1,0:T(1,128)} %bitcast.36), custom_call_target="tpu_custom_call" | custom-call | flops 40000000000 | bytes 1048576 | tf_op jit(solution)/shard_map/combine/pallas_call | solution.py:398
  392.6 2.1 copy.27
  (51 shorter events, 0.5 us)
Async XLA Ops:
  6.5 5.8 %copy-start.6 = (f32[256,512]{1,0:T(8,128)S(1)}, f32[256,512]{1,0:T(8,128)}, u32[]{:S(2)}) copy-start(f32[256,512]{1,0:T(8,128)} %param.33) | copy-start | bytes 1572868
  6.5 6.7 %copy-start.7 = (f32[512,256]{1,0:T(8,128)S(1)}, f32[512,256]{1,0:T(8,128)}, u32[]{:S(2)}) copy-start(f32[512,256]{1,0:T(8,128)} %param.43) | copy-start | bytes 1572868
  6.5 7.4 %copy-start.3 = (f32[256,768]{1,0:T(8,128)S(1)}, f32[256,768]{1,0:T(8,128)}, u32[]{:S(2)}) copy-start(f32[256,768]{1,0:T(8,128)} %param.26) | copy-start | bytes 2359300
  6.5 8.2 %copy-start.4 = (f32[256,768]{1,0:T(8,128)S(1)}, f32[256,768]{1,0:T(8,128)}, u32[]{:S(2)}) copy-start(f32[256,768]{1,0:T(8,128)} %param.27) | copy-start | bytes 2359300
  6.5 222.5 %all-gather.12.cloned.1.call-start = ((), (), s32[]{:S(2)}) async-start(), calls=%async_computation.3 | async-start | bytes 2359296 | tf_op jit(solution)/shard_map/all_gather | solution.py:459
  8.5 7.1 %copy-start.5 = (f32[768,256]{1,0:T(8,128)S(1)}, f32[768,256]{1,0:T(8,128)}, u32[]{:S(2)}) copy-start(f32[768,256]{1,0:T(8,128)} %param.28) | copy-start | bytes 2359300
  8.6 224.9 %all-gather.10.cloned.1.call-start = ((), (), s32[]{:S(2)}) async-start(), calls=%async_computation.2 | async-start | bytes 2359296 | tf_op jit(solution)/shard_map/all_gather | solution.py:459
  10.5 227.6 %all-gather.8.cloned.1.call-start = ((), (), s32[]{:S(2)}) async-start(), calls=%async_computation.1 | async-start | bytes 2359296 | tf_op jit(solution)/shard_map/all_gather | solution.py:459
  12.3 4.1 %copy-start.8 = (f32[512]{0:T(512)S(1)}, f32[512]{0:T(512)}, u32[]{:S(2)}) copy-start(f32[512]{0:T(512)} %param.45) | copy-start | bytes 6148
  12.3 4.1 %copy-start.9 = (f32[512]{0:T(512)S(1)}, f32[512]{0:T(512)}, u32[]{:S(2)}) copy-start(f32[512]{0:T(512)} %param.32) | copy-start | bytes 6148
  12.3 4.1 %copy-start.10 = (f32[512]{0:T(512)S(1)}, f32[512]{0:T(512)}, u32[]{:S(2)}) copy-start(f32[512]{0:T(512)} %param.25) | copy-start | bytes 6148
  12.3 236.5 %all-gather.6.cloned.1.call-start = ((), (), s32[]{:S(2)}) async-start(), calls=%async_computation | async-start | bytes 2359296 | tf_op jit(solution)/shard_map/all_gather | solution.py:459
  13.1 286.4 %all-gather.14.cloned.1.call-start = ((), (), s32[]{:S(2)}) async-start(), calls=%async_computation.4 | async-start | bytes 2359296 | tf_op jit(solution)/shard_map/all_gather | solution.py:459
  161.6 3.7 copy-start.17
  161.6 4.3 %copy-start.1 = (bf16[768,2048]{1,0:T(8,128)(2,1)S(1)}, bf16[768,2048]{1,0:T(8,128)(2,1)}, u32[]{:S(2)}) copy-start(bf16[768,2048]{1,0:T(8,128)(2,1)} %get-tuple-element.14) | copy-start | bytes 9437188
  165.9 6.0 %copy-start.11 = (f32[768]{0:T(1024)S(1)}, f32[768]{0:T(1024)}, u32[]{:S(2)}) copy-start(f32[768]{0:T(1024)} %param.30) | copy-start | bytes 9220
  165.9 6.0 %copy-start.12 = (f32[768]{0:T(1024)S(1)}, f32[768]{0:T(1024)}, u32[]{:S(2)}) copy-start(f32[768]{0:T(1024)} %param.29) | copy-start | bytes 9220
  226.2 2.9 copy-start
  226.2 2.9 copy-start.13
  229.1 4.3 %copy-start.14 = (f32[512]{0:T(512)S(1)}, f32[512]{0:T(512)}, u32[]{:S(2)}) copy-start(f32[512]{0:T(512)} %param.39) | copy-start | bytes 6148
  233.4 4.6 %copy-start.15 = (f32[512]{0:T(512)S(1)}, f32[512]{0:T(512)}, u32[]{:S(2)}) copy-start(f32[512]{0:T(512)} %param.38) | copy-start | bytes 6148
  238.0 10.8 %copy-start.16 = (f32[512]{0:T(512)S(1)}, f32[512]{0:T(512)}, u32[]{:S(2)}) copy-start(f32[512]{0:T(512)} %param.37) | copy-start | bytes 6148
  348.1 2.8 copy-start.2
Sparse Core Ops, SparseCore 0:
  9.5 73.3 all-gather.11
  85.0 64.0 all-gather.9
  151.3 47.8 all-gather.7
  201.2 47.6 all-gather.5
  250.7 48.7 all-gather.13

commit v2 on v1

--- a/solution.py
+++ b/solution.py
@@ -115,6 +115,131 @@
                 self.forward(offset, piece).wait_send()
 
 
+class FsGather:
+    def __init__(self, nfs, ny, pieces, sends, recvs):
+        self.ny, self.nz = ny, nfs // ny
+        self.f = lax.axis_index("fs")
+        self.z, self.y = lax.div(self.f, ny), lax.rem(self.f, ny)
+        self.pieces = pieces
+        self.sends, self.recvs = sends, recvs
+
+    def source(self, p):
+        src, _, _, part, parts, _ = self.pieces[p]
+        step = src.shape[0] // parts
+        return src.at[pl.ds(part * step, step)]
+
+    def place(self, p, index):
+        src, out, dim, part, parts, _ = self.pieces[p]
+        rows, cols = src.shape
+        step = rows // parts
+        if dim == 0:
+            return out.at[pl.ds(pl.multiple_of(index * rows + part * step, step), step)]
+        return out.at[pl.ds(part * step, step), cols_at(index, cols)]
+
+    def move(self, p, kind, index, own, target):
+        block = self.place(p, index)
+        return remote(
+            self.source(p) if own else block, block,
+            self.sends.at[kind, index, p], self.recvs.at[index, p], "fs", target,
+        )
+
+    def arrived(self, p, index):
+        self.move(p, 0, index, False, self.f).wait_recv()
+
+    def along_z(self, p, step, index, own, act):
+        inside = (self.z < self.nz - 1) if step > 0 else (self.z > 0)
+
+        @pl.when(inside)
+        def _():
+            act(self.move(p, 0 if step > 0 else 1, index, own, self.f + step * self.ny))
+
+    def along_y(self, p, index, own, act):
+        for offset in range(1, self.ny):
+            target = self.z * self.ny + lax.rem(self.y + offset, self.ny)
+            act(self.move(p, 1 + offset, index, own, target))
+
+    def others(self, zs):
+        return [zs * self.ny + lax.rem(self.y + offset, self.ny) for offset in range(1, self.ny)]
+
+    def own(self, act, wait):
+        order = range(len(self.pieces))
+        for p in order:
+            self.along_y(p, self.f, True, act)
+            for step in (1, -1):
+                self.along_z(p, step, self.f, True, act)
+        for p in order:
+            if self.pieces[p][5]:
+                for index in self.others(self.z):
+                    if wait:
+                        self.arrived(p, index)
+                    for step in (1, -1):
+                        self.along_z(p, step, index, False, act)
+
+    def relay(self, distance, act, wait):
+        for p in range(len(self.pieces)):
+            for step in (1, -1):
+                zs = self.z - step * distance
+
+                @pl.when(jnp.logical_and(zs >= 0, zs < self.nz))
+                def _():
+                    index = zs * self.ny + self.y
+                    if wait:
+                        self.arrived(p, index)
+                    self.along_z(p, step, index, False, act)
+                    if not self.pieces[p][5]:
+                        self.along_y(p, index, False, act)
+
+        for p in range(len(self.pieces)):
+            if self.pieces[p][5]:
+                for step in (1, -1):
+                    zs = self.z - step * distance
+
+                    @pl.when(jnp.logical_and(zs >= 0, zs < self.nz))
+                    def _():
+                        for index in self.others(zs):
+                            if wait:
+                                self.arrived(p, index)
+                            self.along_z(p, step, index, False, act)
+
+    def start_own(self):
+        self.own(lambda copy: copy.start(), True)
+
+    def start_relay(self, distance):
+        self.relay(distance, lambda copy: copy.start(), True)
+
+    def finish(self):
+        for p in range(len(self.pieces)):
+            if not self.pieces[p][5]:
+                for zs in range(self.nz):
+                    for index in self.others(zs):
+                        self.arrived(p, index)
+        self.own(lambda copy: copy.wait_send(), False)
+        for distance in range(1, self.nz):
+            self.relay(distance, lambda copy: copy.wait_send(), False)
+
+    def greet(self, barrier):
+        ny, z, f = self.ny, self.z, self.f
+        for index in self.others(z):
+            pl.semaphore_signal(barrier, inc=1, device_id={"fs": index}, device_id_type=MESH)
+
+        @pl.when(z > 0)
+        def _():
+            pl.semaphore_signal(barrier, inc=1, device_id={"fs": f - ny}, device_id_type=MESH)
+
+        @pl.when(z < self.nz - 1)
+        def _():
+            pl.semaphore_signal(barrier, inc=1, device_id={"fs": f + ny}, device_id_type=MESH)
+
+        ends = (z > 0).astype(jnp.int32) + (z < self.nz - 1).astype(jnp.int32)
+        return ends + (ny - 1)
+
+    def own_copies(self, sems):
+        return [
+            pltpu.make_async_copy(self.source(p), self.place(p, self.f), sems.at[p])
+            for p in range(len(self.pieces))
+        ]
+
+
 def greet_tp(ntp, barrier):
     t = lax.axis_index("tp")
     for offset in range(1, ntp):
@@ -130,116 +255,46 @@
     own_sem, send_sem, recv_sem, tok_own, tok_send, tok_fwd, tok_recv,
     gain_own, gain_send, gain_fwd, gain_recv,
 ):
-    nz = nfs // ny
-    f = lax.axis_index("fs")
-    z, y = lax.div(f, ny), lax.rem(f, ny)
+    shards = ((gate, gate_out, 0), (up, up_out, 0), (down, down_out, 1))
+    parts = [(*shard, half, 2, i == 0 and half == 0) for i, shard in enumerate(shards) for half in range(2)]
+    weights = FsGather(nfs, ny, parts, send_sem, recv_sem)
     barrier = pltpu.get_barrier_semaphore()
     greet_tp(ntp, barrier)
-    for offset in range(1, ny):
-        other = z * ny + lax.rem(y + offset, ny)
-        pl.semaphore_signal(barrier, inc=1, device_id={"fs": other}, device_id_type=MESH)
-
-    @pl.when(z > 0)
-    def _():
-        pl.semaphore_signal(barrier, inc=1, device_id={"fs": f - ny}, device_id_type=MESH)
-
-    @pl.when(z < nz - 1)
-    def _():
-        pl.semaphore_signal(barrier, inc=1, device_id={"fs": f + ny}, device_id_type=MESH)
-
-    ends = (z > 0).astype(jnp.int32) + (z < nz - 1).astype(jnp.int32)
-    pl.semaphore_wait(barrier, ntp + ny - 2 + ends)
-
-    shards = (gate, up, down)
-    outs = (gate_out, up_out, down_out)
-
-    def place(p, index):
-        if p < 2:
-            return outs[p].at[cols_at(index, shards[p].shape[0])]
-        return outs[p].at[:, cols_at(index, shards[p].shape[1])]
-
-    def along_z(p, step, zs, own):
-        index = zs * ny + y
-        block = place(p, index)
-        kind = 0 if step > 0 else 1
-        return remote(
-            shards[p] if own else block, block, send_sem.at[kind, zs, p],
-            recv_sem.at[index, p], "fs", f + step * ny,
-        )
-
-    def along_y(p, offset, zs, own):
-        index = zs * ny + y
-        block = place(p, index)
-        return remote(
-            shards[p] if own else block, block, send_sem.at[1 + offset, zs, p],
-            recv_sem.at[index, p], "fs", z * ny + lax.rem(y + offset, ny),
-        )
-
-    def arrived(p, index):
-        block = place(p, index)
-        remote(block, block, send_sem.at[0, 0, p], recv_sem.at[index, p], "fs", f).wait_recv()
-
+    pl.semaphore_wait(barrier, weights.greet(barrier) + (ntp - 1))
     toks = TpGather(ntp, tok, tok_out, tok_send, tok_fwd, tok_recv, pieces)
     gain = TpGather(ntp, gains, gains_out, gain_send, gain_fwd, gain_recv, 1)
-    locals_ = [
-        pltpu.make_async_copy(shards[p], place(p, f), own_sem.at[p]) for p in range(3)
-    ]
-    locals_.append(pltpu.make_async_copy(tok, tok_out.at[:, cols_at(toks.t, toks.width)], tok_own))
-    locals_.append(
+    copies = weights.own_copies(own_sem)
+    copies.append(pltpu.make_async_copy(tok, tok_out.at[:, cols_at(toks.t, toks.width)], tok_own))
+    copies.append(
         pltpu.make_async_copy(gains, gains_out.at[:, cols_at(gain.t, gain.width)], gain_own)
     )
-
-    def sends(zs, p, source_step, own, act):
-        for step in (1, -1):
-            if own or step == source_step:
-                inside = (z < nz - 1) if step > 0 else (z > 0)
-
-                @pl.when(inside)
-                def _():
-                    act(along_z(p, step, zs, own))
-
-        for offset in range(1, ny):
-            act(along_y(p, offset, zs, own))
-
-    def all_z(act, wait):
-        for distance in range(1, nz):
-            for p in range(3):
-                for step in (1, -1):
-                    zs = z - step * distance
-
-                    @pl.when(jnp.logical_and(zs >= 0, zs < nz))
-                    def _():
-                        if wait:
-                            arrived(p, zs * ny + y)
-                        sends(zs, p, step, False, act)
-
-    for p in range(3):
-        sends(z, p, 0, True, lambda copy: copy.start())
     gain.start(0)
     for piece in range(pieces):
         toks.start(piece)
-    for copy in locals_:
+    weights.start_own()
+    for copy in copies:
         copy.start()
-    gain.relay()
-    toks.relay()
-    all_z(lambda copy: copy.start(), True)
-    for copy in locals_:
+    for distance in range(1, weights.nz):
+        weights.start_relay(distance)
+        if distance == 1:
+            gain.relay()
+            toks.relay()
+    for copy in copies:
         copy.wait()
     gain.finish()
     toks.finish()
-    for zs in range(nz):
-        for p in range(3):
-            for offset in range(1, ny):
-                arrived(p, zs * ny + lax.rem(y + offset, ny))
-    for p in range(3):
-        sends(z, p, 0, True, lambda copy: copy.wait_send())
-    all_z(lambda copy: copy.wait_send(), False)
+    weights.finish()
 
 
 def reduce_kernel(
-    ntp, pieces, factor, gather,
+    nfs, ntp, ny, pieces, factor, gather, dims,
     part, res, scale, *refs,
 ):
+    count = len(dims)
+    shards, refs = refs[:count], refs[count:]
+    if count:
+        wholes = refs[2 : 2 + count]
+        refs, (w_own, w_send, w_recv) = refs[:2] + refs[2 + count : -3], refs[-3:]
     if gather:
         (out, full, one, pair, two, s1, v1, s2, v2, own_sem, g_send, g_fwd, g_recv) = refs
     else:
@@ -273,12 +328,22 @@
 
     barrier = pltpu.get_barrier_semaphore()
     greet_tp(ntp, barrier)
-    pl.semaphore_wait(barrier, ntp - 1)
+    if count:
+        parts = [(shards[i], wholes[i], dims[i], 0, 1, i == 0) for i in range(count)]
+        weights = FsGather(nfs, ny, parts, w_send, w_recv)
+        pl.semaphore_wait(barrier, weights.greet(barrier) + (ntp - 1))
+    else:
+        pl.semaphore_wait(barrier, ntp - 1)
     for piece in range(pieces):
         for offset in range(1, nx):
             to_partner(offset, piece).start()
     for piece in range(pieces):
         to_partner(0, piece).start()
+    if count:
+        weights.start_own()
+        copies = weights.own_copies(w_own)
+        for copy in copies:
+            copy.start()
     for piece in range(pieces):
         for offset in range(1, nx):
             to_partner(offset, piece).wait_recv()
@@ -301,9 +366,18 @@
     if gather:
         own = pltpu.make_async_copy(out, full.at[:, cols_at(t, width)], own_sem)
         own.start()
+        if count:
+            weights.start_relay(1)
         spread.relay()
+        if count:
+            for distance in range(2, weights.nz):
+                weights.start_relay(distance)
         spread.finish()
         own.wait()
+    if count:
+        for copy in copies:
+            copy.wait()
+        weights.finish()
     for piece in range(pieces):
         for offset in range(nx):
             to_partner(offset, piece).wait_send()
@@ -350,9 +424,12 @@
     return pl.CostEstimate(flops=flops, bytes_accessed=2**20, transcendentals=0)
 
 
+def along_y_of(nfs, ntp):
+    return ntp // 2 if nfs % (ntp // 2) == 0 else 1
+
+
 def enter(nfs, ntp, gate, up, down, tok, gains):
-    ny = ntp // 2 if nfs % (ntp // 2) == 0 else 1
-    nz, nx = nfs // ny, ntp // 2
+    ny, nx = along_y_of(nfs, ntp), ntp // 2
     pieces = tok.shape[0] // LEN
     shape = jax.ShapeDtypeStruct
     return pl.pallas_call(
@@ -367,7 +444,7 @@
         in_specs=[vmem()] * 5,
         out_specs=(anywhere(),) * 5,
         scratch_shapes=[
-            dma(3), dma(ny + 1, nz, 3), dma(nfs, 3),
+            dma(6), dma(ny + 1, nfs, 6), dma(nfs, 6),
             dma(), dma(nx, pieces), dma(nx, pieces), dma(ntp, pieces),
             dma(), dma(nx, 1), dma(nx, 1), dma(ntp, 1),
         ],
@@ -377,7 +454,8 @@
     )(gate, up, down, tok, gains)
 
 
-def combine(ntp, identity, factor, gather, part, res, scale):
+def combine(nfs, ntp, identity, factor, gather, part, res, scale, shards=(), dims=()):
+    ny, count = along_y_of(nfs, ntp), len(dims)
     pieces = res.shape[0] // LEN
     nx = ntp // 2
     rows, width = res.shape
@@ -395,16 +473,22 @@
         out_shape.append(shape((rows, width * ntp), BF16))
         out_specs.append(anywhere())
         scratch += [dma(), dma(nx, pieces), dma(nx, pieces), dma(ntp, pieces)]
+    if count:
+        for shard, dim in zip(shards, dims):
+            grown = [size * (nfs if axis == dim else 1) for axis, size in enumerate(shard.shape)]
+            out_shape.append(shape(tuple(grown), BF16))
+            out_specs.append(anywhere())
+        scratch += [dma(count), dma(ny + 1, nfs, count), dma(nfs, count)]
     return pl.pallas_call(
-        functools.partial(reduce_kernel, ntp, pieces, factor, gather),
+        functools.partial(reduce_kernel, nfs, ntp, ny, pieces, factor, gather, dims),
         out_shape=tuple(out_shape),
-        in_specs=[vmem()] * 3,
+        in_specs=[vmem()] * (3 + count),
         out_specs=tuple(out_specs),
         scratch_shapes=scratch,
         compiler_params=pltpu.CompilerParams(collective_id=identity, has_side_effects=True),
         cost_estimate=cost(4 * 10**10),
         name="combine",
-    )(part, res, scale)
+    )(part, res, scale, *shards)
 
 
 def tables(length, width):
@@ -455,25 +539,23 @@
     scale_query, scale_key, scale_value, scale_outgate,
     ret_gain, decay_rate, w_mix, scale_mix, gain_two,
 ):
-    def gathered(weight, axis):
-        return lax.all_gather(weight.astype(BF16), "fs", axis=axis, tiled=True)
-
-    weights = [gathered(w, 0) for w in (w_query, w_key, w_value, w_outgate)]
-    mix = gathered(w_mix, 1)
+    shards = [w.astype(BF16) for w in (w_query, w_key, w_value, w_outgate, w_mix)]
     gains = jnp.pad(jnp.stack((gain_one, gain_mix, gain_two)), ((0, 5), (0, 0)))
     gate, up, down, full, gains = enter(
         nfs, ntp, w_gate.astype(BF16), w_up.astype(BF16), w_down.astype(BF16), tokens, gains
     )
     part = ffn_part(normed(full, gains[0]), gate, up, down, scale_gate, scale_up)
-    first, full = combine(ntp, 1, 0.5, True, part, tokens, scale_down[None])
+    first, full, *weights, mix = combine(
+        nfs, ntp, 1, 0.5, True, part, tokens, scale_down[None], shards, (0, 0, 0, 0, 1)
+    )
     features = normed(full, gains[1])
     scales = (scale_query, scale_key, scale_value, scale_outgate)
     rows = [(dot(features, w) * s).astype(BF16) for w, s in zip(weights, scales)]
     mixed = retain(*rows, decay_rate, ret_gain)
     part = dot(mixed, mix).astype(BF16)
-    second, full = combine(ntp, 2, 1.0, True, part, first, scale_mix[None])
+    second, full = combine(nfs, ntp, 2, 1.0, True, part, first, scale_mix[None])
     part = ffn_part(normed(full, gains[2]), gate, up, down, scale_gate, scale_up)
-    return combine(ntp, 3, 0.5, False, part, second, scale_down[None])[0]
+    return combine(nfs, ntp, 3, 0.5, False, part, second, scale_down[None])[0]
 
 
 def solution(mesh):

time: 402 us -> 363 us (0.903)
  waiting for transfers between devices: 46.1 us -> 0 us
  Pallas kernels: 262 us -> 285 us
  between operations: 13.3 us -> 0.14 us
  matrix products: 57 us -> 51.3 us
  other arithmetic: 18.1 us -> 22.4 us
    pallas_call x3, Pallas kernels: 111 us -> 178 us  [combine(): pl.pallas_call(functools.partial(reduce_kernel, nfs, ntp, ny, pieces, fac...]
    all_gather x5 -> x0, waiting for transfers between devices: 46 us -> none  [gathered(): return lax.all_gather(weight.astype(BF16), 'fs', axis=axis, tiled=True)]
    pallas_call x1, Pallas kernels: 145 us -> 99.9 us  [enter(): pl.pallas_call(functools.partial(entry_kernel, nfs, ntp, ny, pieces), out...]
    dot_general x9, matrix products: 57 us -> 51.3 us  [dot(): return jnp.dot(left, right, preferred_element_type=F32)]
  transfers between devices with their start and end apart: 5 -> 0, of which waited for: 2 -> 0; matrix products, arithmetic and copies ran while one was open for 12% -> 0% of each run, Pallas kernels for 48% -> 0%
where the time goes in v2:
time: 363 us; the launch traced here: 362 us
  Pallas kernels  285 us (79%)
  matrix products  51.3 us (14%)
  other arithmetic  22.4 us (6%)
  local copies, waits for them, and re-layouts  3.99 us (1%)
    pallas_call x3, Pallas kernels, combine(): pl.pallas_call(functools.partial(reduce_kernel, nfs, ntp, ny, pieces, fac...  178 us
    pallas_call x1, Pallas kernels, enter(): pl.pallas_call(functools.partial(entry_kernel, nfs, ntp, ny, pieces), out...  99.9 us
    dot_general x9, matrix products, dot(): return jnp.dot(left, right, preferred_element_type=F32)  51.3 us
    reduce_sum x3, other arithmetic, normed(): mean = jnp.mean(widened * widened, axis=1, keepdims=True)  8.01 us
    convert_element_type x5, other arithmetic, per_device(): w.astype(BF16)  7.93 us

profile of v2, /device:TPU:0, one launch (start us, length us, event | category | flops | bytes accessed | tf_op | source)
XLA Modules:
  0.0 362.5 jit_solution(18290848518335013200)
XLA Ops:
  0.0 2.0 convert_element_type.71.gate
  2.0 2.0 convert_element_type.72.up
  3.9 1.9 convert_element_type.73.down
  5.9 0.6 select_maximum_fusion.gains
  6.5 99.9 %enter.1 = (bf16[2048,768]{1,0:T(8,128)(2,1)}, bf16[2048,768]{1,0:T(8,128)(2,1)}, bf16[768,2048]{1,0:T(8,128)(2,1)}, bf16[768,2048]{1,0:T(8,128)(2,1)}, f32[8,2048]{1,0:T(8,128)}) custom-call(bf16[256,768]{1,0:T(8,128)(2,1)} %convert_element_type.71.gate, bf16[256,768]{1,0:T(8,128)(2,1)} %convert_element_type.72.up, ...), custom_call_target="tpu_custom_call" | custom-call | flops 99999997952 | bytes 1048576 | tf_op jit(solution)/shard_map/enter/pallas_call | solution.py:435
  106.4 1.1 fusion.25
  107.5 2.6 fusion
  110.1 0.0 copy-start.7
  110.1 5.9 %fusion.15 = f32[768,768]{1,0:T(8,128)} fusion(bf16[2048,768]{1,0:T(8,128)(2,1)} %get-tuple-element.21, bf16[768,2048]{1,0:T(8,128)(2,1)S(1)} %copy-done.1, f32[2048]{0:T(1024)S(1)} %bitcast.28, f32[768]{0:T(1024)S(1)} %add_rsqrt_fusion.2), kind=kOutput, calls=%fused_computation.25 | convolution fusion | flops 2422210560 | bytes 8662016 | tf_op jit(solution)/shard_map/dot_general | solution.py:527
  116.0 11.1 %convolution_convert_fusion.2.part = bf16[768,2048]{1,0:T(8,128)(2,1)} fusion(bf16[768,2048]{1,0:T(8,128)(2,1)} %get-tuple-element.23, f32[768,768]{1,0:T(8,128)} %fusion.15, bf16[2048,768]{1,0:T(8,128)(2,1)} %get-tuple-element.22, f32[768]{0:T(1024)S(1)} %copy-done.7, f32[768]{0:T(1024)S(1)} %copy-done.8, bf16[768,2048]{1,0:T(8,128)(2,1)S(1)} %copy-done.1, ...), kind=kOutput, calls=%fused_computation.17 | convolution fusion | flops 4844421120 | bytes 14959616 | tf_op jit(solution)/shard_map/dot_general | solution.py:527
  127.1 1.8 convert_element_type.78.refs_0_
  128.9 1.8 convert_element_type.79.refs_1_
  130.7 1.8 convert_element_type.80.refs_2_
  132.5 1.8 convert_element_type.81.refs_3_
  134.3 0.7 convert_element_type.82.refs_4_
  135.0 109.6 %combine.3 = (bf16[768,512]{1,0:T(8,128)(2,1)}, bf16[768,2048]{1,0:T(8,128)(2,1)}, bf16[2048,512]{1,0:T(8,128)(2,1)}, bf16[2048,512]{1,0:T(8,128)(2,1)}, bf16[20...) custom-call(bf16[768,2048]{1,0:T(8,128)(2,1)} %convolution_convert_fusion.2.part, ...), custom_call_target="tpu_custom_call" | custom-call | flops 40000000000 | bytes 1048576 | tf_op jit(solution)/shard_map/combine/pallas_call | solution.py:482
  244.7 2.7 fusion.3
  247.4 0.1 copy-done
  247.5 4.5 %multiply_convert_fusion.2.outgate = bf16[768,512]{1,0:T(8,128)(2,1)} fusion(bf16[2048,512]{1,0:T(8,128)(2,1)} %get-tuple-element.28, f32[512]{0:T(512)S(1)} %copy-done.9, bf16[768,2048]{1,0:T(8,128)(2,1)S(1)} %copy-done, f32[2048]{0:T(1024)S(1)} %bitcast.24, f32[768]{0:T(1024)S(1)} %add_rsqrt_fusion.1), kind=kOutput, calls=%fused_computation.20 | convolution fusion | flops 1617690624 | bytes 6042624 | tf_op jit(solution)/shard_map/dot_general | solution.py:527
  252.0 2.8 multiply_convert_fusion.3.value
  254.8 2.7 multiply_convert_fusion.4.key
  257.5 2.7 multiply_convert_fusion.5.query
  260.3 0.6 copy.25.rate
  260.9 7.1 %retain.1 = bf16[768,512]{1,0:T(8,128)(2,1)} custom-call(f32[2,1]{1,0:T(2,128)} %copy.25.rate, bf16[768,512]{1,0:T(8,128)(2,1)} %multiply_convert_fusion.5.query, bf16[768,512]{1,0:T(8,128)(2,1)} %multiply_convert_fusion.4.key, bf16[768,512]{1,0:T(8,128)(2,1)} %multiply_convert_fusion.3.value, bf16[768,512]{1,0:T(8,128)(2,1)} %multiply_convert_fusion.2.outgate, ...), custom_call_target="tpu_custom_call" | custom-call | flops 10000000000 | bytes 1048576 | tf_op jit(solution)/shard_map/retain/pallas_call | solution.py:506
  268.0 4.6 %convolution_convert_fusion.part = bf16[768,2048]{1,0:T(8,128)(2,1)} fusion(bf16[768,512]{1,0:T(8,128)(2,1)} %retain.1, bf16[512,2048]{1,0:T(8,128)(2,1)S(1)} %copy-done.14), kind=kOutput, calls=%fused_computation.15 | convolution fusion | flops 1612185600 | bytes 6029312 | tf_op jit(solution)/shard_map/dot_general | solution.py:527
  272.6 43.3 %combine.4 = (bf16[768,512]{1,0:T(8,128)(2,1)}, bf16[768,2048]{1,0:T(8,128)(2,1)}) custom-call(bf16[768,2048]{1,0:T(8,128)(2,1)} %convolution_convert_fusion.part, bf16[768,512]{1,0:T(8,128)(2,1)} %get-tuple-element.30.res, f32[1,512]{1,0:T(1,128)} %bitcast.34), custom_call_target="tpu_custom_call" | custom-call | flops 40000000000 | bytes 1048576 | tf_op jit(solution)/shard_map/combine/pallas_call | solution.py:482
  315.9 2.7 fusion.6
  318.6 0.1 copy-done.2
  318.7 5.9 %fusion.10 = f32[768,768]{1,0:T(8,128)} fusion(bf16[2048,768]{1,0:T(8,128)(2,1)} %get-tuple-element.21, bf16[768,2048]{1,0:T(8,128)(2,1)S(1)} %copy-done.2, f32[2048]{0:T(1024)S(1)} %bitcast.22, f32[768]{0:T(1024)S(1)} %add_rsqrt_fusion), kind=kOutput, calls=%fused_computation.24 | convolution fusion | flops 2422210560 | bytes 8662016 | tf_op jit(solution)/shard_map/dot_general | solution.py:527
  324.6 11.1 %convolution_convert_fusion.1.part = bf16[768,2048]{1,0:T(8,128)(2,1)} fusion(bf16[768,2048]{1,0:T(8,128)(2,1)} %get-tuple-element.23, f32[768,768]{1,0:T(8,128)} %fusion.10, bf16[2048,768]{1,0:T(8,128)(2,1)} %get-tuple-element.22, f32[768]{0:T(1024)S(1)} %copy-done.7, f32[768]{0:T(1024)S(1)} %copy-done.8, bf16[768,2048]{1,0:T(8,128)(2,1)S(1)} %copy-done.2, ...), kind=kOutput, calls=%fused_computation.16 | convolution fusion | flops 4844421120 | bytes 14959616 | tf_op jit(solution)/shard_map/dot_general | solution.py:527
  335.8 24.7 %combine.5 = bf16[768,512]{1,0:T(8,128)(2,1)} custom-call(bf16[768,2048]{1,0:T(8,128)(2,1)} %convolution_convert_fusion.1.part, bf16[768,512]{1,0:T(8,128)(2,1)} %get-tuple-element.32.res, f32[1,512]{1,0:T(1,128)} %bitcast.36), custom_call_target="tpu_custom_call" | custom-call | flops 40000000000 | bytes 1048576 | tf_op jit(solution)/shard_map/combine/pallas_call | solution.py:482
  360.4 2.1 copy.27
  (36 shorter events, 0.1 us)
Async XLA Ops:
  0.0 5.9 %copy-start.6 = (f32[512]{0:T(512)S(1)}, f32[512]{0:T(512)}, u32[]{:S(2)}) copy-start(f32[512]{0:T(512)} %param.25) | copy-start | bytes 6148
  0.0 5.9 %copy-start.5 = (f32[512]{0:T(512)S(1)}, f32[512]{0:T(512)}, u32[]{:S(2)}) copy-start(f32[512]{0:T(512)} %param.32) | copy-start | bytes 6148
  0.0 5.9 %copy-start.4 = (f32[512]{0:T(512)S(1)}, f32[512]{0:T(512)}, u32[]{:S(2)}) copy-start(f32[512]{0:T(512)} %param.45) | copy-start | bytes 6148
  106.4 3.7 %copy-start.1 = (bf16[768,2048]{1,0:T(8,128)(2,1)S(1)}, bf16[768,2048]{1,0:T(8,128)(2,1)}, u32[]{:S(2)}) copy-start(bf16[768,2048]{1,0:T(8,128)(2,1)} %get-tuple-element.19) | copy-start | bytes 9437188
  110.1 6.0 %copy-start.7 = (f32[768]{0:T(1024)S(1)}, f32[768]{0:T(1024)}, u32[]{:S(2)}) copy-start(f32[768]{0:T(1024)} %param.30) | copy-start | bytes 9220
  110.1 6.0 %copy-start.8 = (f32[768]{0:T(1024)S(1)}, f32[768]{0:T(1024)}, u32[]{:S(2)}) copy-start(f32[768]{0:T(1024)} %param.29) | copy-start | bytes 9220
  127.1 7.2 %copy-start.3 = (f32[512,256]{1,0:T(8,128)S(1)}, f32[512,256]{1,0:T(8,128)}, u32[]{:S(2)}) copy-start(f32[512,256]{1,0:T(8,128)} %param.43) | copy-start | bytes 1572868
  244.7 2.8 copy-start
  244.7 2.8 copy-start.9
  247.5 4.5 %copy-start.10 = (f32[512]{0:T(512)S(1)}, f32[512]{0:T(512)}, u32[]{:S(2)}) copy-start(f32[512]{0:T(512)} %param.39) | copy-start | bytes 6148
  247.5 4.5 %copy-start.17 = (bf16[2048,512]{1,0:T(8,128)(2,1)S(1)}, bf16[2048,512]{1,0:T(8,128)(2,1)}, u32[]{:S(2)}) copy-start(bf16[2048,512]{1,0:T(8,128)(2,1)} %get-tuple-element.27) | copy-start | bytes 6291460
  252.0 2.8 copy-start.11
  252.0 2.8 copy-start.16
  254.8 2.8 copy-start.12
  254.8 2.8 copy-start.15
  257.5 2.7 copy-start.13
  260.9 7.1 %copy-start.14 = (bf16[512,2048]{1,0:T(8,128)(2,1)S(1)}, bf16[512,2048]{1,0:T(8,128)(2,1)}, u32[]{:S(2)}) copy-start(bf16[512,2048]{1,0:T(8,128)(2,1)} %get-tuple-element.29) | copy-start | bytes 6291460
  315.9 2.8 copy-start.2

commit v3 on v2

--- a/solution.py
+++ b/solution.py
@@ -456,7 +456,7 @@
 
 def combine(nfs, ntp, identity, factor, gather, part, res, scale, shards=(), dims=()):
     ny, count = along_y_of(nfs, ntp), len(dims)
-    pieces = res.shape[0] // LEN
+    pieces = res.shape[0] // (LEN // 2)
     nx = ntp // 2
     rows, width = res.shape
     shape = jax.ShapeDtypeStruct

time: 363 us -> 363 us (level)
  no operation moved by 1% of the time
where the time goes in v3:
time: 363 us
  Pallas kernels  285 us (79%)
  matrix products  51.3 us (14%)
  other arithmetic  22.4 us (6%)
  local copies, waits for them, and re-layouts  3.99 us (1%)
    pallas_call x3, Pallas kernels, combine(): pl.pallas_call(functools.partial(reduce_kernel, nfs, ntp, ny, pieces, fac...  178 us
    pallas_call x1, Pallas kernels, enter(): pl.pallas_call(functools.partial(entry_kernel, nfs, ntp, ny, pieces), out...  99.9 us
    dot_general x9, matrix products, dot(): return jnp.dot(left, right, preferred_element_type=F32)  51.3 us
    reduce_sum x3, other arithmetic, normed(): mean = jnp.mean(widened * widened, axis=1, keepdims=True)  8.01 us
    convert_element_type x5, other arithmetic, per_device(): w.astype(BF16)  7.93 us

profile of v3, /device:TPU:0, one launch (start us, length us, event | category | flops | bytes accessed | tf_op | source)
XLA Modules:
  0.0 362.8 jit_solution(4823830145280718028)
XLA Ops:
  0.0 2.0 convert_element_type.71.gate
  2.0 2.0 convert_element_type.72.up
  3.9 1.9 convert_element_type.73.down
  5.9 0.6 select_maximum_fusion.gains
  6.5 99.9 %enter.1 = (bf16[2048,768]{1,0:T(8,128)(2,1)}, bf16[2048,768]{1,0:T(8,128)(2,1)}, bf16[768,2048]{1,0:T(8,128)(2,1)}, bf16[768,2048]{1,0:T(8,128)(2,1)}, f32[8,2048]{1,0:T(8,128)}) custom-call(bf16[256,768]{1,0:T(8,128)(2,1)} %convert_element_type.71.gate, bf16[256,768]{1,0:T(8,128)(2,1)} %convert_element_type.72.up, ...), custom_call_target="tpu_custom_call" | custom-call | flops 99999997952 | bytes 1048576 | tf_op jit(solution)/shard_map/enter/pallas_call | solution.py:435
  106.4 1.1 fusion.25
  107.5 2.6 fusion
  110.1 0.0 copy-start.8
  110.1 5.9 %fusion.15 = f32[768,768]{1,0:T(8,128)} fusion(bf16[2048,768]{1,0:T(8,128)(2,1)} %get-tuple-element.21, bf16[768,2048]{1,0:T(8,128)(2,1)S(1)} %copy-done.1, f32[2048]{0:T(1024)S(1)} %bitcast.28, f32[768]{0:T(1024)S(1)} %add_rsqrt_fusion.2), kind=kOutput, calls=%fused_computation.25 | convolution fusion | flops 2422210560 | bytes 8662016 | tf_op jit(solution)/shard_map/dot_general | solution.py:527
  116.0 11.1 %convolution_convert_fusion.2.part = bf16[768,2048]{1,0:T(8,128)(2,1)} fusion(bf16[768,2048]{1,0:T(8,128)(2,1)} %get-tuple-element.23, f32[768,768]{1,0:T(8,128)} %fusion.15, bf16[2048,768]{1,0:T(8,128)(2,1)} %get-tuple-element.22, f32[768]{0:T(1024)S(1)} %copy-done.7, f32[768]{0:T(1024)S(1)} %copy-done.8, bf16[768,2048]{1,0:T(8,128)(2,1)S(1)} %copy-done.1, ...), kind=kOutput, calls=%fused_computation.17 | convolution fusion | flops 4844421120 | bytes 14959616 | tf_op jit(solution)/shard_map/dot_general | solution.py:527
  127.1 1.8 convert_element_type.78.refs_0_
  128.9 1.8 convert_element_type.79.refs_1_
  130.7 1.8 convert_element_type.80.refs_2_
  132.5 1.8 convert_element_type.81.refs_3_
  134.3 0.7 convert_element_type.82.refs_4_
  135.0 110.0 %combine.3 = (bf16[768,512]{1,0:T(8,128)(2,1)}, bf16[768,2048]{1,0:T(8,128)(2,1)}, bf16[2048,512]{1,0:T(8,128)(2,1)}, bf16[2048,512]{1,0:T(8,128)(2,1)}, bf16[20...) custom-call(bf16[768,2048]{1,0:T(8,128)(2,1)} %convolution_convert_fusion.2.part, ...), custom_call_target="tpu_custom_call" | custom-call | flops 40000000000 | bytes 1048576 | tf_op jit(solution)/shard_map/combine/pallas_call | solution.py:482
  245.1 2.7 fusion.3
  247.8 0.1 copy-done
  247.9 4.5 %multiply_convert_fusion.2.outgate = bf16[768,512]{1,0:T(8,128)(2,1)} fusion(bf16[2048,512]{1,0:T(8,128)(2,1)} %get-tuple-element.28, f32[512]{0:T(512)S(1)} %copy-done.9, bf16[768,2048]{1,0:T(8,128)(2,1)S(1)} %copy-done, f32[2048]{0:T(1024)S(1)} %bitcast.24, f32[768]{0:T(1024)S(1)} %add_rsqrt_fusion.1), kind=kOutput, calls=%fused_computation.20 | convolution fusion | flops 1617690624 | bytes 6042624 | tf_op jit(solution)/shard_map/dot_general | solution.py:527
  252.4 2.8 multiply_convert_fusion.3.value
  255.2 2.8 multiply_convert_fusion.4.key
  257.9 2.7 multiply_convert_fusion.5.query
  260.7 0.6 copy.25.rate
  261.3 7.1 %retain.1 = bf16[768,512]{1,0:T(8,128)(2,1)} custom-call(f32[2,1]{1,0:T(2,128)} %copy.25.rate, bf16[768,512]{1,0:T(8,128)(2,1)} %multiply_convert_fusion.5.query, bf16[768,512]{1,0:T(8,128)(2,1)} %multiply_convert_fusion.4.key, bf16[768,512]{1,0:T(8,128)(2,1)} %multiply_convert_fusion.3.value, bf16[768,512]{1,0:T(8,128)(2,1)} %multiply_convert_fusion.2.outgate, ...), custom_call_target="tpu_custom_call" | custom-call | flops 10000000000 | bytes 1048576 | tf_op jit(solution)/shard_map/retain/pallas_call | solution.py:506
  268.4 4.6 %convolution_convert_fusion.part = bf16[768,2048]{1,0:T(8,128)(2,1)} fusion(bf16[768,512]{1,0:T(8,128)(2,1)} %retain.1, bf16[512,2048]{1,0:T(8,128)(2,1)S(1)} %copy-done.14), kind=kOutput, calls=%fused_computation.15 | convolution fusion | flops 1612185600 | bytes 6029312 | tf_op jit(solution)/shard_map/dot_general | solution.py:527
  273.0 43.2 %combine.4 = (bf16[768,512]{1,0:T(8,128)(2,1)}, bf16[768,2048]{1,0:T(8,128)(2,1)}) custom-call(bf16[768,2048]{1,0:T(8,128)(2,1)} %convolution_convert_fusion.part, bf16[768,512]{1,0:T(8,128)(2,1)} %get-tuple-element.30.res, f32[1,512]{1,0:T(1,128)} %bitcast.34), custom_call_target="tpu_custom_call" | custom-call | flops 40000000000 | bytes 1048576 | tf_op jit(solution)/shard_map/combine/pallas_call | solution.py:482
  316.3 2.7 fusion.6
  319.0 0.1 copy-done.2
  319.1 5.9 %fusion.10 = f32[768,768]{1,0:T(8,128)} fusion(bf16[2048,768]{1,0:T(8,128)(2,1)} %get-tuple-element.21, bf16[768,2048]{1,0:T(8,128)(2,1)S(1)} %copy-done.2, f32[2048]{0:T(1024)S(1)} %bitcast.22, f32[768]{0:T(1024)S(1)} %add_rsqrt_fusion), kind=kOutput, calls=%fused_computation.24 | convolution fusion | flops 2422210560 | bytes 8662016 | tf_op jit(solution)/shard_map/dot_general | solution.py:527
  325.0 11.1 %convolution_convert_fusion.1.part = bf16[768,2048]{1,0:T(8,128)(2,1)} fusion(bf16[768,2048]{1,0:T(8,128)(2,1)} %get-tuple-element.23, f32[768,768]{1,0:T(8,128)} %fusion.10, bf16[2048,768]{1,0:T(8,128)(2,1)} %get-tuple-element.22, f32[768]{0:T(1024)S(1)} %copy-done.7, f32[768]{0:T(1024)S(1)} %copy-done.8, bf16[768,2048]{1,0:T(8,128)(2,1)S(1)} %copy-done.2, ...), kind=kOutput, calls=%fused_computation.16 | convolution fusion | flops 4844421120 | bytes 14959616 | tf_op jit(solution)/shard_map/dot_general | solution.py:527
  336.2 24.6 %combine.5 = bf16[768,512]{1,0:T(8,128)(2,1)} custom-call(bf16[768,2048]{1,0:T(8,128)(2,1)} %convolution_convert_fusion.1.part, bf16[768,512]{1,0:T(8,128)(2,1)} %get-tuple-element.32.res, f32[1,512]{1,0:T(1,128)} %bitcast.36), custom_call_target="tpu_custom_call" | custom-call | flops 40000000000 | bytes 1048576 | tf_op jit(solution)/shard_map/combine/pallas_call | solution.py:482
  360.7 2.1 copy.27
  (36 shorter events, 0.1 us)
Async XLA Ops:
  0.0 5.9 %copy-start.6 = (f32[512]{0:T(512)S(1)}, f32[512]{0:T(512)}, u32[]{:S(2)}) copy-start(f32[512]{0:T(512)} %param.25) | copy-start | bytes 6148
  0.0 5.9 %copy-start.5 = (f32[512]{0:T(512)S(1)}, f32[512]{0:T(512)}, u32[]{:S(2)}) copy-start(f32[512]{0:T(512)} %param.32) | copy-start | bytes 6148
  0.0 5.9 %copy-start.4 = (f32[512]{0:T(512)S(1)}, f32[512]{0:T(512)}, u32[]{:S(2)}) copy-start(f32[512]{0:T(512)} %param.45) | copy-start | bytes 6148
  106.4 3.7 %copy-start.1 = (bf16[768,2048]{1,0:T(8,128)(2,1)S(1)}, bf16[768,2048]{1,0:T(8,128)(2,1)}, u32[]{:S(2)}) copy-start(bf16[768,2048]{1,0:T(8,128)(2,1)} %get-tuple-element.19) | copy-start | bytes 9437188
  110.1 6.0 %copy-start.7 = (f32[768]{0:T(1024)S(1)}, f32[768]{0:T(1024)}, u32[]{:S(2)}) copy-start(f32[768]{0:T(1024)} %param.30) | copy-start | bytes 9220
  110.1 6.0 %copy-start.8 = (f32[768]{0:T(1024)S(1)}, f32[768]{0:T(1024)}, u32[]{:S(2)}) copy-start(f32[768]{0:T(1024)} %param.29) | copy-start | bytes 9220
  127.1 7.2 %copy-start.3 = (f32[512,256]{1,0:T(8,128)S(1)}, f32[512,256]{1,0:T(8,128)}, u32[]{:S(2)}) copy-start(f32[512,256]{1,0:T(8,128)} %param.43) | copy-start | bytes 1572868
  245.1 2.8 copy-start
  245.1 2.8 copy-start.9
  247.9 4.5 %copy-start.10 = (f32[512]{0:T(512)S(1)}, f32[512]{0:T(512)}, u32[]{:S(2)}) copy-start(f32[512]{0:T(512)} %param.39) | copy-start | bytes 6148
  247.9 4.5 %copy-start.17 = (bf16[2048,512]{1,0:T(8,128)(2,1)S(1)}, bf16[2048,512]{1,0:T(8,128)(2,1)}, u32[]{:S(2)}) copy-start(bf16[2048,512]{1,0:T(8,128)(2,1)} %get-tuple-element.27) | copy-start | bytes 6291460
  252.4 2.8 copy-start.11
  252.4 2.8 copy-start.16
  255.2 2.8 copy-start.12
  255.2 2.8 copy-start.15
  257.9 2.7 copy-start.13
  261.3 7.1 %copy-start.14 = (bf16[512,2048]{1,0:T(8,128)(2,1)S(1)}, bf16[512,2048]{1,0:T(8,128)(2,1)}, u32[]{:S(2)}) copy-start(bf16[512,2048]{1,0:T(8,128)(2,1)} %get-tuple-element.29) | copy-start | bytes 6291460
  316.3 2.8 copy-start.2
